TPU v7x, 256 devices: a whole 4x4x8 slice. The times are simulated.
256 devices in a mesh: fs: 32 (over z, x), tp: 8 (over y, core).
Axes of the slice: x: 4, y: 4, z: 8, core: 2. Of those that a mesh axis runs over, the one named last changes fastest.
Arguments:
- tokens: bfloat16 [32768, 2048], P(('fs', 'tp')), may hold values from -6 to 6
- gate_pre: bfloat16 [32768, 5632], P('fs', 'tp'), may hold values from -6 to 6
- value_pre: bfloat16 [32768, 5632], P('fs', 'tp'), may hold values from -6 to 6
- up_gate_w: bfloat16 [2048, 5632], P('fs', 'tp'), may hold values from -0.078125 to 0.078125
- up_value_w: bfloat16 [2048, 5632], P('fs', 'tp'), may hold values from -0.078125 to 0.078125
- conv_weight: float32 [3, 5632], P(None, 'tp'), may hold values from -3 to 3
- conv_bias: float32 [5632], P('tp'), may hold values from -3 to 3
- hidden_grad: bfloat16 [32768, 5632], P('fs', 'tp'), may hold values from -6 to 6
Outputs:
- input_grad: bfloat16 [32768, 2048], P(('fs', 'tp'))
- up_gate_grad: float32 [2048, 5632], P('fs', 'tp')
- up_value_grad: float32 [2048, 5632], P('fs', 'tp')
- conv_weight_grad: float32 [3, 5632], P(None, 'tp')
- conv_bias_grad: float32 [5632], P('tp')
All inputs are finite; a program needn't handle non-finite values.
Results may differ from a plain program's by a relative error of at most 0.013.
Values may be sent and summed in bfloat16 or wider, within the bound.
A program may use at most 128 MiB of HBM per device.

v0:
```python
import jax
import jax.numpy as jnp
from jax import lax
from jax.sharding import Mesh
from jax.sharding import PartitionSpec as P

FS = ("fs_0", "fs_1")
FS_TP = ("fs_0", "fs_1", "tp")


def copy_for_each(shard, axis):
    peers = lax.axis_size(axis)
    return lax.all_to_all(
        jnp.broadcast_to(shard[None], (peers, *shard.shape)), axis, 0, 0, tiled=True
    )


def taken_together(shard, axis):
    return copy_for_each(shard, axis).sum(axis=0)


def in_one_piece(arrays, axis, dim, along):
    ends, at = ([], 0)
    for a in arrays[:-1]:
        at += a.shape[along]
        ends.append(at)
    both = jnp.concatenate(arrays, axis=along)
    return tuple(jnp.split(lax.all_gather(both, axis, axis=dim, tiled=True), ends, axis=along))


def summed_rows(subtotal, axes):
    for axis in axes:
        subtotal = lax.psum_scatter(subtotal, axis, scatter_dimension=0, tiled=True)
    return subtotal


def in_blocks(shard, dim, peers):
    lengths = shard.shape
    blocks = shard.reshape(*lengths[:dim], peers, lengths[dim] // peers, *lengths[dim + 1 :])
    return jnp.moveaxis(blocks, dim, 0)


def summed_on_arrival(shard, axis, dim):
    blocks = in_blocks(shard, dim, lax.axis_size(axis))
    arrived = lax.all_to_all(blocks, axis, split_axis=0, concat_axis=0, tiled=True)
    return arrived.astype(jnp.float32).sum(axis=0)


def contract_rows(left, right):
    return lax.dot_general(
        left, right, (((0,), (0,)), ((), ())), preferred_element_type=jnp.float32
    )


def contract_cols(left, right):
    return lax.dot_general(
        left, right, (((1,), (1,)), ((), ())), preferred_element_type=jnp.float32
    )


def on_device(
    tokens, gate_pre, value_pre, up_gate_w, up_value_w, conv_weight, conv_bias, hidden_grad
):
    length = gate_pre.shape[0]
    col_count = gate_pre.shape[1]
    scale = float(length * lax.axis_size(FS)) ** (-0.5)
    gate_float = gate_pre.astype(jnp.float32)
    padded = jnp.pad(gate_float, ((2, 0), (0, 0)))
    gate_conv = (
        conv_bias
        + conv_weight[0] * padded[:length]
        + conv_weight[1] * padded[1 : length + 1]
        + conv_weight[2] * padded[2:]
    )
    active, gelu_back = jax.vjp(jax.nn.gelu, gate_conv)
    grad_float = hidden_grad.astype(jnp.float32)
    value_grad = (grad_float * active).astype(jnp.bfloat16)
    conv_grad = gelu_back(grad_float * value_pre.astype(jnp.float32))[0]
    shifted = jnp.pad(conv_grad, ((0, 2), (0, 0)))
    gate_grad = (
        conv_weight[2] * conv_grad
        + conv_weight[1] * shifted[1 : length + 1]
        + conv_weight[0] * shifted[2:]
    ).astype(jnp.bfloat16)
    conv_terms = jnp.stack(
        [
            jnp.sum(conv_grad * padded[:length], axis=0),
            jnp.sum(conv_grad * padded[1 : length + 1], axis=0),
            jnp.sum(conv_grad * padded[2:], axis=0),
            jnp.sum(conv_grad, axis=0),
        ]
    )
    conv_total = taken_together(conv_terms, FS) * scale
    whole_tokens = lax.all_gather(tokens, "tp", axis=0, tiled=True)
    full_gate, full_value = in_one_piece((up_gate_w, up_value_w), FS, 0, 1)
    joined = summed_rows(
        jnp.concatenate(
            [contract_rows(whole_tokens, gate_grad), contract_rows(whole_tokens, value_grad)],
            axis=1,
        ),
        FS,
    )
    gate_out = joined[:, :col_count] * scale
    value_out = joined[:, col_count:] * scale
    input_grad = summed_on_arrival(
        (contract_cols(gate_grad, full_gate) + contract_cols(value_grad, full_value)).astype(
            jnp.bfloat16
        ),
        "tp",
        0,
    ).astype(jnp.bfloat16)
    return (input_grad, gate_out, value_out, conv_total[:3], conv_total[3])


def solution(mesh):
    finer = Mesh(mesh.devices.reshape(8, 4, mesh.shape["tp"]), ("fs_0", "fs_1", "tp"))
    in_specs = (
        P(FS_TP, None),
        P(FS, "tp"),
        P(FS, "tp"),
        P(FS, "tp"),
        P(FS, "tp"),
        P(None, "tp"),
        P("tp"),
        P(FS, "tp"),
    )
    out_specs = (P(FS_TP, None), P(FS, "tp"), P(FS, "tp"), P(None, "tp"), P("tp"))
    return jax.shard_map(
        on_device, mesh=finer, in_specs=in_specs, out_specs=out_specs, check_vma=False
    )
```

profile of v0, /device:TPU:8, one launch (start us, length us, event | category | flops | bytes accessed | tf_op | source)
XLA Modules:
  0.0 301.7 jit_solution(17411305977214108581)
XLA Ops:
  7.2 0.0 copy-start
  7.2 0.0 copy-start.7
  7.2 0.0 copy-start.2
  7.2 0.0 copy-start.8
  7.2 0.0 all-gather.5.cloned.1.call-start
  7.3 0.7 all-gather.5.cloned.1.call-update
  7.9 0.0 all-gather.3.cloned.1.call-start
  8.0 1.8 pad_maximum_fusion.1
  9.8 0.0 all-gather.3.cloned.1.call-update
  9.8 0.0 reduce-scatter.5.cloned.1.call-start
  9.9 0.0 copy-start.3
  9.9 1.8 convert_element_type.26
  11.7 0.0 copy-done.7
  11.8 0.0 copy-done
  11.8 0.0 copy-done.2
  11.8 0.0 copy-done.8
  11.8 0.0 copy-done.3
  11.8 6.5 %multiply_reduce_fusion.2 = (f32[704]{0:T(1024)S(1)}, f32[704]{0:T(1024)S(1)}, f32[704]{0:T(1024)S(1)}, f32[704]{0:T(1024)S(1)}, f32[1024,704]{0,1:T(8,128)S(1)}, /*index=5*/f32[1024,704]{0,1:T(8,128)}) fusion(f32[1024,704]{0,1:T(8,128)S(1)} %convert_element_type.26, bf16[1024,704]{0,1:T(8,128)(2,1)S(1)} %copy-done, bf16[1024,704]{0,1:T(8,128)(2,1)S(1)} %copy-done.2, ...), kind=kLoop, calls=%fused_computation.29 | loop fusion | flops 25949440 | bytes 12998656 | tf_op jit(solution)/shard_map/reduce_sum | solution.py:87
  18.3 3.0 %fusion.6 = bf16[1024,704]{0,1:T(8,128)(2,1)} fusion(f32[1024,704]{0,1:T(8,128)S(1)} %get-tuple-element.32, f32[704]{0:T(1024)S(1)} %get-tuple-element.30, f32[704]{0:T(1024)S(1)} %get-tuple-element.31, f32[704]{0:T(1024)S(1)} %get-tuple-element.29), kind=kLoop, calls=%fused_computation.18 | loop fusion | flops 4325376 | bytes 4333824 | tf_op jit(solution)/shard_map/convert_element_type | solution.py:84
  21.4 25.0 %all-gather.5.cloned.1.call-done = bf16[1024,2048]{1,0:T(8,128)(2,1)} async-done(((bf16[128,2048]{1,0:T(8,128)(2,1)}), bf16[1024,2048]{1,0:T(8,128)(2,1)}) %all-gather.5.cloned.1.call-update) | async-done | bytes 4194320 | tf_op jit(solution)/shard_map/all_gather | solution.py:94
  46.4 8.4 %convolution_bitcast_fusion.1 = f32[2048,704]{0,1:T(8,128)} fusion(bf16[1024,704]{0,1:T(8,128)(2,1)} %fusion.6, bf16[1024,2048]{1,0:T(8,128)(2,1)} %all-gather.5.cloned.1.call-done), kind=kOutput, calls=%fused_computation.5 | convolution fusion | flops 2952790016 | bytes 11403264 | tf_op jit(solution)/shard_map/dot_general | solution.py:50
  54.8 0.0 copy-done.1
  54.8 5.3 %convolution_bitcast_fusion = f32[2048,704]{0,1:T(8,128)} fusion(bf16[1024,2048]{1,0:T(8,128)(2,1)S(1)} %copy-done.10, bf16[1024,704]{0,1:T(8,128)(2,1)S(1)} %copy-done.4, f32[1024,704]{0,1:T(8,128)S(1)} %copy-done.1), kind=kOutput, calls=%fused_computation.4 | convolution fusion | flops 2960719872 | bytes 14286848 | tf_op jit(solution)/shard_map/dot_general | solution.py:50
  60.1 10.8 %pad_maximum_fusion = f32[2048,1408]{0,1:T(8,128)} fusion(f32[2048,704]{0,1:T(8,128)} %convolution_bitcast_fusion, f32[2048,704]{0,1:T(8,128)} %convolution_bitcast_fusion.1), kind=kLoop, calls=%fused_computation | loop fusion | flops 2883584 | bytes 23068672 | tf_op jit(solution)/shard_map/concatenate | solution.py:97
  70.9 0.0 reduce-scatter.5.cloned.1.call-update
  71.0 0.8 broadcast_in_dim.2
  71.8 10.0 %all-to-all-start.1 = ((f32[32,4,704]{2,1,0:T(4,128)}), f32[32,4,704]{2,1,0:T(4,128)S(1)}, u32[]{:S(2)}, u32[]{:S(2)}) async-start(f32[32,4,704]{2,1,0:T(4,128)} %broadcast_in_dim.2), calls=%async_computation.2 | async-start | bytes 786432 | tf_op jit(solution)/shard_map/all_to_all | solution.py:13
  81.8 56.8 %all-gather.3.cloned.1.call-done = bf16[2048,1408]{1,0:T(8,128)(2,1)} async-done(((bf16[64,1408]{1,0:T(8,128)(2,1)}), bf16[2048,1408]{1,0:T(8,128)(2,1)}) %all-gather.3.cloned.1.call-update) | async-done | bytes 5767184 | tf_op jit(solution)/shard_map/all_gather | solution.py:28
  138.7 6.0 %fusion.1 = f32[1024,2048]{1,0:T(8,128)S(1)} fusion(bf16[1024,704]{0,1:T(8,128)(2,1)} %fusion.6, bf16[2048,1408]{1,0:T(8,128)(2,1)} %all-gather.3.cloned.1.call-done), kind=kOutput, calls=%fused_computation.13 | convolution fusion | flops 2952790016 | bytes 12976128 | tf_op jit(solution)/shard_map/dot_general | solution.py:56
  144.7 0.0 copy-done.5
  144.7 0.0 copy-done.9
  144.7 7.6 %add_convert_fusion = bf16[1024,2048]{1,0:T(8,128)(2,1)} fusion(f32[1024,2048]{1,0:T(8,128)S(1)} %fusion.1, bf16[2048,1408]{1,0:T(8,128)(2,1)S(1)} %copy-done.9, bf16[1024,704]{0,1:T(8,128)(2,1)S(1)} %copy-done.5, f32[1024,704]{0,1:T(8,128)S(1)} %copy-done.1), kind=kOutput, calls=%fused_computation.1 | convolution fusion | flops 2964914176 | bytes 20054016 | tf_op jit(solution)/shard_map/dot_general | solution.py:56
  152.3 0.0 all-to-all-done.1
  152.3 5.0 %all-to-all-start = ((bf16[8,128,2048]{2,1,0:T(8,128)(2,1)}), bf16[8,128,2048]{2,1,0:T(8,128)(2,1)}, u32[]{:S(2)}, u32[]{:S(2)}) async-start(bf16[8,128,2048]{2,1,0:T(8,128)(2,1)} %bitcast.11), calls=%async_computation | async-start | bytes 8388608 | tf_op jit(solution)/shard_map/all_to_all | solution.py:45
  157.3 105.4 %reduce-scatter.5.cloned.1.call-done = f32[256,1408]{0,1:T(8,128)} async-done(((f32[2048,1408]{0,1:T(8,128)}), f32[256,1408]{0,1:T(8,128)}) %reduce-scatter.5.cloned.1.call-update) | async-done | bytes 1441808 | tf_op jit(solution)/shard_map/reduce_scatter | solution.py:33
  262.6 2.9 copy.22
  265.5 0.0 reduce-scatter.7.cloned.1.call-update
  265.6 0.1 reduce_sum.62
  265.7 0.0 copy-start.6
  265.7 0.6 slice_reduce_fusion
  266.3 0.0 all-to-all-done
  266.3 3.8 %reduce_sum.57 = bf16[128,2048]{1,0:T(8,128)(2,1)} reduce(bf16[8,128,2048]{2,1,0:T(8,128)(2,1)} %all-to-all-done, bf16[]{:T(256)} %constant.19.clone.1), dimensions={0}, to_apply=%region_0.1 | reduce | flops 1835008 | bytes 4718594 | tf_op jit(solution)/shard_map/reduce_sum | solution.py:46
  270.1 21.8 %reduce-scatter.7.cloned.1.call-done = f32[64,1408]{1,0:T(8,128)} async-done(((f32[256,1408]{1,0:T(8,128)}), f32[64,1408]{1,0:T(8,128)}) %reduce-scatter.7.cloned.1.call-update) | async-done | bytes 360464
  292.0 1.1 fusion.18
  293.1 0.2 copy.25
  293.3 0.8 copy.20
  294.1 0.2 copy.26
  294.3 0.8 copy.21
  (18 shorter events, 0.2 us)
Async XLA Ops:
  7.2 4.6 %copy-start = (bf16[1024,704]{0,1:T(8,128)(2,1)S(1)}, bf16[1024,704]{0,1:T(8,128)(2,1)}, u32[]{:S(2)}) copy-start(bf16[1024,704]{0,1:T(8,128)(2,1)} %param.9) | copy-start | bytes 4325380
  7.2 4.5 %copy-start.7 = (f32[3,704]{1,0:T(4,128)S(1)}, f32[3,704]{1,0:T(4,128)}, u32[]{:S(2)}) copy-start(f32[3,704]{1,0:T(4,128)} %param.13) | copy-start | bytes 25348
  7.2 4.6 %copy-start.2 = (bf16[1024,704]{0,1:T(8,128)(2,1)S(1)}, bf16[1024,704]{0,1:T(8,128)(2,1)}, u32[]{:S(2)}) copy-start(bf16[1024,704]{0,1:T(8,128)(2,1)} %param.10) | copy-start | bytes 4325380
  7.2 4.6 %copy-start.8 = (f32[704]{0:T(1024)S(1)}, f32[704]{0:T(1024)}, u32[]{:S(2)}) copy-start(f32[704]{0:T(1024)} %param.14) | copy-start | bytes 8452
  7.2 39.2 %all-gather.5.cloned.1.call-start = ((), (), s32[]{:S(2)}) async-start(), calls=%async_computation.5 | async-start | bytes 4718592 | tf_op jit(solution)/shard_map/all_gather | solution.py:94
  7.9 130.7 %all-gather.3.cloned.1.call-start = ((), (), s32[]{:S(2)}) async-start(), calls=%async_computation.4 | async-start | bytes 5947392 | tf_op jit(solution)/shard_map/all_gather | solution.py:28
  9.8 252.8 %reduce-scatter.5.cloned.1.call-start = ((), (), s32[]{:S(2)}) async-start(), calls=%async_computation.6 | async-start | bytes 12976128 | tf_op jit(solution)/shard_map/reduce_scatter | solution.py:33
  9.9 1.9 copy-start.3
  21.4 33.4 %copy-start.1 = (f32[1024,704]{0,1:T(8,128)S(1)}, f32[1024,704]{0,1:T(8,128)}, u32[]{:S(2)}) copy-start(f32[1024,704]{0,1:T(8,128)} %get-tuple-element.33) | copy-start | bytes 8650756
  46.4 8.4 %copy-start.4 = (bf16[1024,704]{0,1:T(8,128)(2,1)S(1)}, bf16[1024,704]{0,1:T(8,128)(2,1)}, u32[]{:S(2)}) copy-start(bf16[1024,704]{0,1:T(8,128)(2,1)} %param.15) | copy-start | bytes 4325380
  46.4 8.4 %copy-start.10 = (bf16[1024,2048]{1,0:T(8,128)(2,1)S(1)}, bf16[1024,2048]{1,0:T(8,128)(2,1)}, u32[]{:S(2)}) copy-start(bf16[1024,2048]{1,0:T(8,128)(2,1)} %all-gather.5.cloned.1.call-done) | copy-start | bytes 12582916
  71.8 80.4 %all-to-all-start.1 = ((f32[32,4,704]{2,1,0:T(4,128)}), f32[32,4,704]{2,1,0:T(4,128)S(1)}, u32[]{:S(2)}, u32[]{:S(2)}) async-start(f32[32,4,704]{2,1,0:T(4,128)} %broadcast_in_dim.2), calls=%async_computation.2 | async-start | bytes 786432 | tf_op jit(solution)/shard_map/all_to_all | solution.py:13
  138.7 6.0 %copy-start.5 = (bf16[1024,704]{0,1:T(8,128)(2,1)S(1)}, bf16[1024,704]{0,1:T(8,128)(2,1)}, u32[]{:S(2)}) copy-start(bf16[1024,704]{0,1:T(8,128)(2,1)} %param.15) | copy-start | bytes 4325380
  138.7 6.0 %copy-start.9 = (bf16[2048,1408]{1,0:T(8,128)(2,1)S(1)}, bf16[2048,1408]{1,0:T(8,128)(2,1)}, u32[]{:S(2)}) copy-start(bf16[2048,1408]{1,0:T(8,128)(2,1)} %all-gather.3.cloned.1.call-done) | copy-start | bytes 17301508
  152.3 114.0 %all-to-all-start = ((bf16[8,128,2048]{2,1,0:T(8,128)(2,1)}), bf16[8,128,2048]{2,1,0:T(8,128)(2,1)}, u32[]{:S(2)}, u32[]{:S(2)}) async-start(bf16[8,128,2048]{2,1,0:T(8,128)(2,1)} %bitcast.11), calls=%async_computation | async-start | bytes 8388608 | tf_op jit(solution)/shard_map/all_to_all | solution.py:45
  157.3 134.7 %reduce-scatter.7.cloned.1.call-start = ((), (), s32[]{:S(2)}) async-start(), calls=%async_computation.7 | async-start | bytes 1802240
  265.7 27.6 %copy-start.6 = (f32[4,704]{1,0:T(4,128)}, f32[4,704]{1,0:T(4,128)S(1)}, u32[]{:S(2)}) copy-start(f32[4,704]{1,0:T(4,128)S(1)} %broadcast_multiply_fusion.2) | copy-start | bytes 33796
Sparse Core Ops, SparseCore 0:
  9.9 36.4 all-gather.4
  49.5 89.0 all-gather.2
  141.2 121.3 reduce-scatter.4
  265.7 26.2 reduce-scatter.6
where the time goes:
time: 302 us
  waiting for transfers between devices  210 us (70%)
  other arithmetic  28 us (9%)
  matrix products  27.3 us (9%)
  starting transfers between devices  15.1 us (5%)
  between operations  14 us (5%)
  local copies, waits for them, and re-layouts  7.54 us (2%)
    reduce_scatter x1, waiting for transfers between devices, summed_rows(): subtotal = lax.psum_scatter(subtotal, axis, scatter_dimension=0, tiled=True)  105 us
    all_gather x1, waiting for transfers between devices, in_one_piece(): lax.all_gather(both, axis, axis=dim, tiled=True)  56.8 us
    all_gather x1, waiting for transfers between devices, on_device(): whole_tokens = lax.all_gather(tokens, 'tp', axis=0, tiled=True)  25 us
    unnamed x5, waiting for transfers between devices  22.5 us
    dot_general x2, matrix products, contract_rows(): lax.dot_general(left, right, (((0,), (0,)), ((), ())), preferred_element_...  13.7 us
    dot_general x2, matrix products, contract_cols(): lax.dot_general(left, right, (((1,), (1,)), ((), ())), preferred_element_...  13.6 us
    concatenate x1, other arithmetic, on_device(): jnp.concatenate([contract_rows(whole_tokens, gate_grad), contract_rows(wh...  10.8 us
    all_to_all x1, starting transfers between devices, copy_for_each(): lax.all_to_all(jnp.broadcast_to(shard[None], (peers, *shard.shape)), axis...  10 us
  transfers between devices with their start and end apart: 6, of which 4 were waited for; matrix products, arithmetic and copies ran while one was open for 20% of the time, Pallas kernels for 0%

commit v1 on v0

v1 whole, which is shorter than its diff:
```python
import functools

import jax
import jax.numpy as jnp
from jax import lax
from jax.experimental import pallas as pl
from jax.experimental.pallas import tpu as pltpu
from jax.sharding import PartitionSpec as P

MESH = pl.DeviceIdType.MESH
F32 = jnp.float32
BF16 = jnp.bfloat16
NC = 2
SUB = 64
LANES = 128

LINK = 46_650.0
TWIN = 300_000.0
HOP = 2.2
TWIN_HOP = 1.0


class Plan:
    def __init__(self):
        self.messages = {}
        self.tasks = {}

    def message(self, name, link, source, target, device, nbytes):
        self.messages[name] = (link, source, target, device, nbytes)

    def task(self, name, rank, cost, body=None, waits=(), after=(), sends=()):
        self.tasks[name] = (rank, cost, body, tuple(waits), tuple(after), tuple(sends))

    def order(self):
        arrival, free, ended, listed = {}, {}, {}, []
        left = dict(self.tasks)
        now = 0.0
        while left:
            best = None
            for name, (rank, cost, body, waits, after, sends) in left.items():
                if any(w not in arrival for w in waits) or any(a not in ended for a in after):
                    continue
                ready = max([now] + [arrival[w] for w in waits])
                key = (ready > now, ready if ready > now else 0.0, rank)
                if best is None or key < best[0]:
                    best = (key, name, ready)
            name, ready = best[1], best[2]
            rank, cost, body, waits, after, sends = left.pop(name)
            now = ready + cost
            ended[name] = now
            listed.append(name)
            for m in sends:
                link, nbytes = self.messages[m][0], self.messages[m][4]
                start = max(now, free.get(link, 0.0))
                rate, hop = (TWIN, TWIN_HOP) if link == "twin" else (LINK, HOP)
                free[link] = start + nbytes / rate
                arrival[m] = free[link] + hop
        self.length = now
        self.ended = ended
        return listed


def nbytes_of(ref):
    size = ref.dtype.itemsize
    for s in ref.shape:
        size *= s
    return size


def kernel(
    dims,
    tokens,
    gate_in,
    value_in,
    wg_in,
    wv_in,
    cw_in,
    cb_in,
    hidden_in,
    ig_out,
    gg_out,
    vg_out,
    cwg_out,
    cbg_out,
    gate,
    value,
    hidden,
    wgs,
    wvs,
    cw,
    cb,
    tok,
    wa,
    wb,
    ga,
    gb,
    pa,
    pb,
    az_up,
    az_dn,
    ax_up,
    ax_dn,
    bx_up,
    bx_dn,
    bz_up,
    bz_dn,
    igp,
    twin_in,
    y_up,
    y_dn,
    later,
    terms,
    cx,
    cz,
    load_sem,
    send_sem,
    recv_sem,
):
    nz, nx, ny = dims
    fs, tp = lax.axis_index("fs"), lax.axis_index("tp")
    z, x, y, c = fs // nx, fs % nx, tp // NC, tp % NC
    rows, width = gate.shape
    mine = tok.shape[0] // (ny * NC)
    whole = width // LANES * LANES
    rest = width - whole
    shard = wgs.shape[0]
    group = nx * shard
    scale = float(rows * nz * nx) ** (-0.5)

    def at_z(d):
        return (((z + d + nz) % nz) * nx + x, tp)

    def at_x(d):
        return (z * nx + (x + d + nx) % nx, tp)

    def at_y(d):
        return (fs, ((y + d + ny) % ny) * NC + c)

    twin = (fs, y * NC + 1 - c)

    loads = {}
    for i, (name, source, target) in enumerate(
        (
            ("wg", wg_in, wgs),
            ("wv", wv_in, wvs),
            ("tok", tokens, tok.at[pl.ds(tp * mine, mine)]),
            ("gate", gate_in, gate),
            ("value", value_in, value),
            ("hidden", hidden_in, hidden),
            ("cw", cw_in, cw),
            ("cb", cb_in, cb),
        )
    ):
        loads[name] = pltpu.make_async_copy(source, target, load_sem.at[i])
        loads[name].start()
    barrier = pltpu.get_barrier_semaphore()
    peers = (at_z(1), at_z(-1), at_x(1), at_x(-1), at_y(1), at_y(-1), twin)
    for peer in peers:
        pl.semaphore_signal(barrier, inc=1, device_id=peer, device_id_type=MESH)

    loads["wg"].wait()
    loads["wv"].wait()
    wa[fs] = wgs[:, :whole]
    wb[fs, :, :whole] = wvs[:, :whole]
    wb[fs, :, whole:] = jnp.concatenate(
        [wvs[:, whole:].astype(F32), wgs[:, whole:].astype(F32)], axis=1
    ).astype(BF16)
    later[...] = jnp.zeros_like(later)
    terms[...] = jnp.zeros_like(terms)
    pl.semaphore_wait(barrier, len(peers))

    plan = Plan()

    def ring_at(axis):
        return {
            "z": (nz, z, at_z),
            "x": (nx, x, at_x),
            "y": (ny, y, at_y),
        }[axis]

    def gather(name, axis, block, half, rank, extra=None, first=None):
        n, me, to = ring_at(axis)
        far = n // 2

        def idx(d):
            return (me + d + n) % n

        for h in range(1, far + 1):
            up, dn = idx(1 - h), idx(h - 1)
            su, sd = (block(up), block(dn)) if h < far else (half(up, 0), half(dn, 1))
            plan.message(f"{name}.up{h}", axis + "+", su, su, to(1), nbytes_of(su))
            plan.message(f"{name}.dn{h}", axis + "-", sd, sd, to(-1), nbytes_of(sd))
        ends = {0: first}
        for h in range(1, far):
            for way, sign in (("up", -1), ("dn", 1)):
                task = f"{name}.{way}{h}"
                plan.task(
                    task,
                    rank,
                    0.05,
                    waits=[task],
                    sends=[f"{name}.{way}{h + 1}"] + (extra(sign * h) if extra else []),
                )
                ends[sign * h] = task
        plan.task(
            f"{name}.last",
            rank,
            0.05,
            waits=[f"{name}.up{far}", f"{name}.dn{far}"],
            sends=extra(far) if extra else [],
        )
        ends[far] = f"{name}.last"
        return [f"{name}.up1", f"{name}.dn1"], ends

    def scatter(name, axis, block, half, up_in, dn_in, half_in, rank, cost, ready, last, then=()):
        n, me, to = ring_at(axis)
        far = n // 2

        def idx(d):
            return (me + d + n) % n

        for j in range(1, far + 1):
            up, dn = idx(j), idx(-j)
            if j == far:
                su, tu = half(up, 0), half_in(up_in, j - 1, 0)
                sd, td = half(dn, 1), half_in(dn_in, j - 1, 1)
            else:
                su, tu, sd, td = block(up), up_in.at[j - 1], block(dn), dn_in.at[j - 1]
            plan.message(f"{name}.up{j}", axis + "+", su, tu, to(1), nbytes_of(su))
            plan.message(f"{name}.dn{j}", axis + "-", sd, td, to(-1), nbytes_of(sd))
        plan.task(
            f"{name}.start", rank, 0.02, after=ready(far), sends=[f"{name}.up{far}", f"{name}.dn{far}"]
        )
        for j in range(far - 1, 0, -1):
            for way, sign, h, came in (("up", 1, 0, up_in), ("dn", -1, 1, dn_in)):
                at = idx(sign * j)

                def add(at=at, j=j, h=h, came=came):
                    if j + 1 == far:
                        own, other = half(at, h), half_in(came, j, h)
                    else:
                        own, other = block(at), came.at[j]
                    own[...] = (own[...].astype(F32) + other[...].astype(F32)).astype(BF16)

                plan.task(
                    f"{name}.{way}{j}",
                    rank,
                    cost,
                    add,
                    waits=[f"{name}.{way}{j + 1}"],
                    after=ready(sign * j),
                    sends=[f"{name}.{way}{j}"],
                )
        own = block(me)

        def end():
            last(own[...].astype(F32) + up_in[0].astype(F32) + dn_in[0].astype(F32))

        plan.task(
            f"{name}.end",
            rank,
            cost * 1.5,
            end,
            waits=[f"{name}.up1", f"{name}.dn1"],
            after=ready(0),
            sends=then,
        )

    offsets_z = [0] + [s * h for h in range(1, nz // 2) for s in (-1, 1)] + [nz // 2]

    ax_first, ax_ends = gather(
        "wax", "x", lambda i: wa.at[z * nx + i], lambda i, h: wa.at[z * nx + i, pl.ds(h * shard // 2, shard // 2)], 0
    )
    az_first, az_ends = gather(
        "waz",
        "z",
        lambda i: wa.at[pl.ds(i * nx, nx)],
        lambda i, h: wa.at[pl.ds(i * nx + h * (nx // 2), nx // 2)],
        1,
    )
    plan.task("waz.go", 0, 0.02, after=[t for t in ax_ends.values() if t], sends=az_first)
    az_ends[0] = "waz.go"
    bx_first, bx_ends = {}, {}
    for d in offsets_z:
        bx_first[d], bx_ends[d] = gather(
            f"wbx{d}",
            "x",
            lambda i, d=d: wb.at[((z + d + nz) % nz) * nx + i],
            lambda i, h, d=d: wb.at[((z + d + nz) % nz) * nx + i, pl.ds(h * shard // 2, shard // 2)],
            2,
        )
    bz_first, bz_ends = gather(
        "wbz",
        "z",
        lambda i: wb.at[i * nx + x],
        lambda i, h: wb.at[i * nx + x, pl.ds(h * shard // 2, shard // 2)],
        0,
        extra=lambda d: bx_first[d],
    )

    def tok_at(i):
        return tok.at[pl.ds((i * NC + c) * mine, mine)]

    for d in range(-(ny // 2) + 1, ny // 2 + 1):
        block = tok_at((y + d + ny) % ny)
        plan.message(f"twin{d}", "twin", block, block, twin, nbytes_of(block))
    tok_first, tok_ends = gather(
        "tok",
        "y",
        tok_at,
        lambda i, h: tok.at[pl.ds((i * NC + c) * mine + h * (mine // 2), mine // 2)],
        0,
        extra=lambda d: [f"twin{d}"],
    )
    plan.task("tok.own", 0, 0.02, lambda: loads["tok"].wait(), sends=tok_first + ["twin0"])
    plan.task("go", -1, 0.02, sends=ax_first + bz_first + bx_first[0])
    plan.task(
        "tok.all",
        3,
        0.02,
        waits=[f"twin{d}" for d in range(-(ny // 2) + 1, ny // 2 + 1)],
        after=[t for t in tok_ends.values() if t] + ["tok.own"],
    )

    k0 = 0.7978845608028654
    k1 = k0 * 0.044715

    def act_step(row, col, size, write):
        r = pl.ds(row, SUB)
        cols = pl.ds(col, size)
        g = gate[r, cols].astype(F32)
        before = gate[pl.ds(pl.multiple_of(jnp.maximum(row - 16, 0), 16), 16), cols].astype(F32)[8:]
        before = jnp.where(row > 0, before, 0.0)
        both = jnp.concatenate([before, g], axis=0)
        one = pltpu.roll(both, 1, 0)[8:]
        two = pltpu.roll(both, 2, 0)[8:]
        w0, w1, w2 = cw[0:1, cols], cw[1:2, cols], cw[2:3, cols]
        conv = cb[0:1, cols] + w0 * two + w1 * one + w2 * g
        square = conv * conv
        t = jnp.tanh(conv * (k0 + k1 * square))
        cdf = 0.5 + 0.5 * t
        slope = cdf + conv * (0.5 - 0.5 * (t * t)) * (k0 + (3.0 * k1) * square)
        hg = hidden[r, cols].astype(F32)
        vg = hg * (conv * cdf)
        cg = slope * (hg * value[r, cols].astype(F32))
        after = jnp.concatenate([cg, later[:, cols]], axis=0)
        gg = (
            w2 * cg
            + w1 * pltpu.roll(after, SUB + 7, 0)[:SUB]
            + w0 * pltpu.roll(after, SUB + 6, 0)[:SUB]
        )
        later[:, cols] = cg[:8]
        for k, term in enumerate((cg * two, cg * one, cg * g, cg)):
            terms[k, :, cols] += term.reshape(SUB // 8, 8, size).sum(axis=0)
        write(r, cols, gg, vg)

    def write_whole(r, cols, gg, vg):
        ga[r, cols] = gg.astype(BF16)
        gb[r, cols] = vg.astype(BF16)

    def write_rest(r, cols, gg, vg):
        gb[r, whole:] = jnp.concatenate([vg, gg], axis=1).astype(BF16)

    n_act = 8 if rows >= 8 * SUB else rows // SUB
    per_act = rows // n_act // SUB

    def act(k):
        if k == 0:
            for name in ("gate", "value", "hidden", "cw", "cb"):
                loads[name].wait()

        def sub(i, carry):
            row = pl.multiple_of(rows - (k * per_act + i + 1) * SUB, SUB)

            def col(j, carry):
                act_step(row, pl.multiple_of(j * LANES, LANES), LANES, write_whole)
                return carry

            lax.fori_loop(0, whole // LANES, col, 0)
            act_step(row, whole, rest, write_rest)
            return carry

        lax.fori_loop(0, per_act, sub, 0)

    for k in range(n_act):
        plan.task(f"act{k}", 5, 1.1, functools.partial(act, k), after=[f"act{k - 1}"] if k else [])
    acted = f"act{n_act - 1}"

    def conv_start():
        sums = [terms[k].sum(axis=0, keepdims=True) for k in range(4)]
        cx[x] = jnp.concatenate(sums + [jnp.zeros((4, width), F32)], axis=0)

    def ring_of_slots(name, axis, slots):
        n, me, to = ring_at(axis)
        names = []
        for h in range(1, n // 2 + 1):
            for way, sign in (("up", 1), ("dn", -1)):
                if h == n // 2 and sign < 0:
                    continue
                s = slots.at[(me + sign * (1 - h) + n) % n]
                m = f"{name}.{way}{h}"
                plan.message(m, axis + ("+" if sign > 0 else "-"), s, s, to(sign), nbytes_of(s))
                nxt = [f"{name}.{way}{h + 1}"] if h + 1 < n // 2 or (h + 1 == n // 2 and sign > 0) else []
                plan.task(m, 4, 0.05, waits=[m], sends=nxt)
                names.append(m)
        firsts = [f"{name}.up1"] + ([f"{name}.dn1"] if n > 2 else [])
        return firsts, names

    cx_first, cx_names = ring_of_slots("cx", "x", cx)
    cz_first, cz_names = ring_of_slots("cz", "z", cz)

    def conv_middle():
        total = cx[0]
        for i in range(1, nx):
            total = total + cx[i]
        cz[z] = total

    def conv_end():
        total = cz[0]
        for i in range(1, nz):
            total = total + cz[i]
        total = total * scale
        cwg_out[...] = total[:3]
        cbg_out[...] = total[3:4]

    plan.task("conv.start", 6, 0.2, conv_start, after=[acted], sends=cx_first)
    plan.task("conv.middle", 6, 0.1, conv_middle, after=cx_names + ["conv.start"], sends=cz_first)
    plan.task("conv.end", 9, 0.1, conv_end, after=cz_names + ["conv.middle"])

    grad_order = [nz // 2] + [s * h for h in range(nz // 2 - 1, 0, -1) for s in (1, -1)] + [0]

    def grad(d):
        to_z = (z + d + nz) % nz
        left = tok[:, pl.ds(pl.multiple_of(to_z * group, group), group)]
        over_rows = (((0,), (0,)), ((), ()))
        for right, out in ((ga, pa), (gb, pb)):
            part = lax.dot_general(left, right[...], over_rows, preferred_element_type=F32)
            out[to_z] = part.astype(BF16).reshape(nx, shard, part.shape[1])

    for d in grad_order:
        plan.task(f"grad{d}", 7, 1.1, functools.partial(grad, d), after=["tok.all", acted])

    def ax_last(total):
        gg_out[:, :whole] = total * scale

    def az_last(total):
        pa[z] = total.astype(BF16)

    scatter(
        "pax",
        "x",
        lambda i: pa.at[z, i],
        lambda i, h: pa.at[z, i, pl.ds(h * shard // 2, shard // 2)],
        ax_up,
        ax_dn,
        lambda ref, j, h: ref.at[j, pl.ds(h * shard // 2, shard // 2)],
        3,
        0.1,
        lambda d: ["paz.end"],
        ax_last,
    )
    scatter(
        "paz",
        "z",
        lambda i: pa.at[i],
        lambda i, h: pa.at[i, pl.ds(h * (nx // 2), nx // 2)],
        az_up,
        az_dn,
        lambda ref, j, h: ref.at[j, pl.ds(h * (nx // 2), nx // 2)],
        2,
        0.25,
        lambda d: [f"grad{d}"],
        az_last,
    )

    def bz_last(total):
        total = total * scale
        vg_out[...] = total[:, :width]
        gg_out[:, whole:] = total[:, width:]

    def bx_last(d, total):
        pb[(z + d + nz) % nz, x] = total.astype(BF16)

    for i, d in enumerate(grad_order):
        scatter(
            f"pbx{d}",
            "x",
            lambda i, d=d: pb.at[(z + d + nz) % nz, i],
            lambda i, h, d=d: pb.at[(z + d + nz) % nz, i, pl.ds(h * shard // 2, shard // 2)],
            bx_up.at[i],
            bx_dn.at[i],
            lambda ref, j, h: ref.at[j, pl.ds(h * shard // 2, shard // 2)],
            2,
            0.1,
            lambda e, d=d: [f"grad{d}"],
            functools.partial(bx_last, d),
        )
    scatter(
        "pbz",
        "z",
        lambda i: pb.at[i, x],
        lambda i, h: pb.at[i, x, pl.ds(h * shard // 2, shard // 2)],
        bz_up,
        bz_dn,
        lambda ref, j, h: ref.at[j, pl.ds(h * shard // 2, shard // 2)],
        2,
        0.1,
        lambda d: [f"pbx{d}.end"],
        bz_last,
    )

    over_cols = (((1,), (1,)), ((), ()))

    def ig(d):
        at = (z + d + nz) % nz
        left_w = wa[pl.ds(at * nx, nx)].reshape(group, whole)
        right_w = wb[pl.ds(at * nx, nx)].reshape(group, 2 * width - whole)
        part = lax.dot_general(ga[...], left_w, over_cols, preferred_element_type=F32)
        part = part + lax.dot_general(gb[...], right_w, over_cols, preferred_element_type=F32)
        part = part.astype(BF16)
        for k in range(ny * NC):
            igp[at, k % NC, k // NC] = part[k * mine : (k + 1) * mine]

    for d in offsets_z:
        at = (z + d + nz) % nz
        m = f"igt{d}"
        source, target = igp.at[at, 1 - c], twin_in.at[at]
        plan.message(m, "twin", source, target, twin, nbytes_of(source))
        ends = [t for t in (az_ends[d], bz_ends[d], *bx_ends[d].values()) if t]
        plan.task(f"ig{d}", 8, 1.1, functools.partial(ig, d), after=[acted] + ends, sends=[m])

        def merge(at=at):
            igp[at, c] = (igp[at, c].astype(F32) + twin_in[at].astype(F32)).astype(BF16)

        plan.task(f"igm{d}", 3, 0.2, merge, waits=[m], after=[f"ig{d}"])

        def ig_last(total, at=at):
            ig_out[:, pl.ds(pl.multiple_of(at * group, group), group)] = total.astype(BF16)

        scatter(
            f"igy{d}",
            "y",
            lambda i, at=at: igp.at[at, c, i],
            lambda i, h, at=at: igp.at[at, c, i, pl.ds(h * (mine // 2), mine // 2)],
            y_up.at[at],
            y_dn.at[at],
            lambda ref, j, h: ref.at[j, pl.ds(h * (mine // 2), mine // 2)],
            3,
            0.05,
            lambda e, d=d: [f"igm{d}"],
            ig_last,
        )

    copies = {}
    number = {name: i for i, name in enumerate(plan.messages)}
    for name, (link, source, target, device, size) in plan.messages.items():
        i = number[name]
        copies[name] = pltpu.make_async_remote_copy(
            src_ref=source,
            dst_ref=target,
            send_sem=send_sem.at[i],
            recv_sem=recv_sem.at[i],
            device_id=device,
            device_id_type=MESH,
        )
    for name in plan.order():
        rank, cost, body, waits, after, sends = plan.tasks[name]
        for m in waits:
            copies[m].wait_recv()
        if body is not None:
            body()
        for m in sends:
            copies[m].start()
    for m in plan.messages:
        copies[m].wait_send()


def on_device(dims, *args):
    tokens, gate_pre, value_pre, up_gate_w, up_value_w, conv_weight, conv_bias, hidden_grad = args
    nz, nx, ny = dims
    rows, width = gate_pre.shape
    mine, model = tokens.shape
    shard = up_gate_w.shape[0]
    whole = width // LANES * LANES
    ca, cb = whole, 2 * width - whole
    group = nx * shard
    shape = jax.ShapeDtypeStruct
    out = pl.pallas_call(
        functools.partial(kernel, dims),
        out_shape=(
            shape((mine, model), BF16),
            shape((shard, width), F32),
            shape((shard, width), F32),
            shape((3, width), F32),
            shape((1, width), F32),
        ),
        in_specs=[pl.BlockSpec(memory_space=pl.ANY)] * 8,
        out_specs=[pl.BlockSpec(memory_space=pltpu.VMEM)] * 5,
        scratch_shapes=[
            pltpu.VMEM((rows, width), BF16),
            pltpu.VMEM((rows, width), BF16),
            pltpu.VMEM((rows, width), BF16),
            pltpu.VMEM((shard, width), BF16),
            pltpu.VMEM((shard, width), BF16),
            pltpu.VMEM((3, width), F32),
            pltpu.VMEM((1, width), F32),
            pltpu.VMEM((mine * ny * NC, model), BF16),
            pltpu.VMEM((nz * nx, shard, ca), BF16),
            pltpu.VMEM((nz * nx, shard, cb), BF16),
            pltpu.VMEM((rows, ca), BF16),
            pltpu.VMEM((rows, cb), BF16),
            pltpu.VMEM((nz, nx, shard, ca), BF16),
            pltpu.VMEM((nz, nx, shard, cb), BF16),
            pltpu.VMEM((nz // 2, nx, shard, ca), BF16),
            pltpu.VMEM((nz // 2, nx, shard, ca), BF16),
            pltpu.VMEM((nx // 2, shard, ca), BF16),
            pltpu.VMEM((nx // 2, shard, ca), BF16),
            pltpu.VMEM((nz, nx // 2, shard, cb), BF16),
            pltpu.VMEM((nz, nx // 2, shard, cb), BF16),
            pltpu.VMEM((nz // 2, shard, cb), BF16),
            pltpu.VMEM((nz // 2, shard, cb), BF16),
            pltpu.VMEM((nz, NC, ny, mine, group), BF16),
            pltpu.VMEM((nz, ny, mine, group), BF16),
            pltpu.VMEM((nz, ny // 2, mine, group), BF16),
            pltpu.VMEM((nz, ny // 2, mine, group), BF16),
            pltpu.VMEM((8, width), F32),
            pltpu.VMEM((4, 8, width), F32),
            pltpu.VMEM((nx, 8, width), F32),
            pltpu.VMEM((nz, 8, width), F32),
            pltpu.SemaphoreType.DMA((8,)),
            pltpu.SemaphoreType.DMA((192,)),
            pltpu.SemaphoreType.DMA((192,)),
        ],
        compiler_params=pltpu.CompilerParams(
            collective_id=0, has_side_effects=True, vmem_limit_bytes=64_000_000
        ),
    )(
        tokens,
        gate_pre,
        value_pre,
        up_gate_w,
        up_value_w,
        conv_weight,
        conv_bias.reshape(1, width),
        hidden_grad,
    )
    return (out[0], out[1], out[2], out[3], out[4].reshape(width))


def solution(mesh):
    sizes = (mesh.shape["fs"], mesh.shape["tp"])
    dims = {(32, 8): (8, 4, 4)}[sizes]
    in_specs = (
        P(("fs", "tp"), None),
        P("fs", "tp"),
        P("fs", "tp"),
        P("fs", "tp"),
        P("fs", "tp"),
        P(None, "tp"),
        P("tp"),
        P("fs", "tp"),
    )
    out_specs = (P(("fs", "tp"), None), P("fs", "tp"), P("fs", "tp"), P(None, "tp"), P("tp"))
    return jax.shard_map(
        functools.partial(on_device, dims),
        mesh=mesh,
        in_specs=in_specs,
        out_specs=out_specs,
        check_vma=False,
    )
```

time: 302 us -> 104 us (0.34)
  waiting for transfers between devices: 210 us -> 0 us
  Pallas kernels: 0 us -> 88.3 us
  matrix products: 27.3 us -> 0 us
  other arithmetic: 28 us -> 1.32 us
  starting transfers between devices: 15.1 us -> 0 us
  between operations: 14 us -> 0.67 us
  local copies, waits for them, and re-layouts: 7.54 us -> 11.9 us
    reduce_scatter x1 -> x0, waiting for transfers between devices: 105 us -> none  [summed_rows(): subtotal = lax.psum_scatter(subtotal, axis, scatter_dimension=0, tiled=True)]
    pallas_call x0 -> x1, Pallas kernels: none -> 88.3 us  [on_device(): pl.pallas_call(functools.partial(kernel, dims), out_shape=(shape((mine, m...]
    all_gather x2 -> x0, waiting for transfers between devices: 81.8 us -> none  [the longest x1 56.8 us: in_one_piece(): lax.all_gather(both, axis, axis=dim, tiled=True)]
    dot_general x4 -> x0, matrix products: 27.3 us -> none  [the longest x2 13.7 us: contract_rows(): lax.dot_general(left, right, (((0,), (0,)), ((), ())), preferred_element_...]
    unnamed x5 -> x0, waiting for transfers between devices: 22.5 us -> none
    all_to_all x2 -> x0, starting transfers between devices: 15 us -> none  [the longest x1 10 us: copy_for_each(): lax.all_to_all(jnp.broadcast_to(shard[None], (peers, *shard.shape)), axis...]
    concatenate x2 -> x0, other arithmetic: 12.6 us -> none  [the longest x1 10.8 us: on_device(): jnp.concatenate([contract_rows(whole_tokens, gate_grad), contract_rows(wh...]
    reduce_sum x3 -> x0, other arithmetic: 10.5 us -> none  [the longest x1 6.53 us: on_device(): jnp.sum(conv_grad * padded[:length], axis=0)]
  transfers between devices with their start and end apart: 6 -> 0, of which waited for: 4 -> 0; matrix products, arithmetic and copies ran while one was open for 20% -> 0% of each run, Pallas kernels for 0% -> 0%
where the time goes in v1:
time: 104 us; the launch traced here: 102 us
  Pallas kernels  88.3 us (85%)
  local copies, waits for them, and re-layouts  11.9 us (11%)
  other arithmetic  1.32 us (1%)
    pallas_call x1, Pallas kernels, on_device(): pl.pallas_call(functools.partial(kernel, dims), out_shape=(shape((mine, m...  88.3 us
    unnamed x15, local copies, waits for them, and re-layouts  10.5 us

profile of v1, /device:TPU:8, one launch (start us, length us, event | category | flops | bytes accessed | tf_op | source)
XLA Modules:
  0.0 102.2 jit_solution(2171657014689172519)
XLA Ops:
  0.6 0.0 copy-start
  0.6 1.4 %reshape.16.cb_in = f32[1,704]{1,0:T(1,128)} reshape(f32[704]{0:T(1024)} %param.14) | data formatting | bytes 5632 | tf_op jit(solution)/shard_map/reshape | solution.py:644
  2.0 2.6 %copy.13.gate_in = bf16[1024,704]{1,0:T(8,128)(2,1)} copy(bf16[1024,704]{0,1:T(8,128)(2,1)} %param.9) | data formatting | bytes 2883584 | tf_op args[1]
  4.6 0.0 copy-done
  4.6 0.0 copy-start.1
  4.6 1.6 %copy.14.value_in = bf16[1024,704]{1,0:T(8,128)(2,1)} copy(bf16[1024,704]{0,1:T(8,128)(2,1)S(1)} %copy-done) | data formatting | bytes 2883584 | tf_op args[2]
  6.2 0.0 copy-done.1
  6.2 1.6 %copy.15.hidden_in = bf16[1024,704]{1,0:T(8,128)(2,1)} copy(bf16[1024,704]{0,1:T(8,128)(2,1)S(1)} %copy-done.1) | data formatting | bytes 2883584 | tf_op args[7]
  7.7 88.3 %shard_map.119 = (bf16[128,2048]{1,0:T(8,128)(2,1)}, f32[64,704]{1,0:T(8,128)}, f32[64,704]{1,0:T(8,128)}, f32[3,704]{1,0:T(4,128)}, f32[1,704]{1,0:T(1,128)}) custom-call(bf16[128,2048]{1,0:T(8,128)(2,1)} %tokens.1, bf16[1024,704]{1,0:T(8,128)(2,1)} %copy.13.gate_in, bf16[1024,704]{1,0:T(8,128)(2,1)} %copy.14.value_in, bf16[64,704]{1,0:T(8,128)(2,1)} %wg_in.1, ...), custom_call_target="tpu_custom_call" | custom-call | tf_op jit(solution)/shard_map/pallas_call | solution.py:588
  96.1 0.0 copy-start.2
  96.1 0.0 copy-start.3
  96.1 1.3 %reduce = f32[704]{0:T(1024)} reduce(f32[1,704]{1,0:T(1,128)} %get-tuple-element.14, f32[]{:T(128)} %constant.1), dimensions={0}, to_apply=%get-tuple-element.14.reduce_sub_computation | reduce | bytes 5636 | tf_op jit(solution)/shard_map/pallas_call | solution.py:588
  97.4 1.9 %copy.20 = bf16[128,2048]{1,0:T(8,128)(2,1)} copy(bf16[128,2048]{1,0:T(8,128)(2,1)} %get-tuple-element.20) | data formatting | bytes 1048576
  99.3 1.6 %copy.21 = f32[64,704]{1,0:T(8,128)} copy(f32[64,704]{1,0:T(8,128)} %get-tuple-element.21) | data formatting | bytes 360448
  100.9 0.0 copy-done.2
  100.9 0.7 copy.22
  101.6 0.0 copy-done.3
  101.6 0.6 copy.23
Async XLA Ops:
  0.6 4.0 %copy-start = (bf16[1024,704]{0,1:T(8,128)(2,1)S(1)}, bf16[1024,704]{0,1:T(8,128)(2,1)}, u32[]{:S(2)}) copy-start(bf16[1024,704]{0,1:T(8,128)(2,1)} %param.10) | copy-start | bytes 4325380
  4.6 1.6 %copy-start.1 = (bf16[1024,704]{0,1:T(8,128)(2,1)S(1)}, bf16[1024,704]{0,1:T(8,128)(2,1)}, u32[]{:S(2)}) copy-start(bf16[1024,704]{0,1:T(8,128)(2,1)} %param.15) | copy-start | bytes 4325380
  96.1 4.8 %copy-start.2 = (f32[64,704]{1,0:T(8,128)S(1)}, f32[64,704]{1,0:T(8,128)}, u32[]{:S(2)}) copy-start(f32[64,704]{1,0:T(8,128)} %get-tuple-element.22) | copy-start | bytes 540676
  96.1 5.5 %copy-start.3 = (f32[3,704]{1,0:T(4,128)S(1)}, f32[3,704]{1,0:T(4,128)}, u32[]{:S(2)}) copy-start(f32[3,704]{1,0:T(4,128)} %get-tuple-element.23) | copy-start | bytes 25348

commit v2 on v1

--- a/solution.py
+++ b/solution.py
@@ -11,7 +11,7 @@
 F32 = jnp.float32
 BF16 = jnp.bfloat16
 NC = 2
-SUB = 64
+SUB = 16
 LANES = 128
 
 LINK = 46_650.0
@@ -92,8 +92,7 @@
     tok,
     wa,
     wb,
-    ga,
-    gb,
+    gt,
     pa,
     pb,
     az_up,
@@ -108,7 +107,8 @@
     twin_in,
     y_up,
     y_dn,
-    later,
+    taps,
+    coef,
     terms,
     cx,
     cz,
@@ -119,10 +119,11 @@
     nz, nx, ny = dims
     fs, tp = lax.axis_index("fs"), lax.axis_index("tp")
     z, x, y, c = fs // nx, fs % nx, tp // NC, tp % NC
-    rows, width = gate.shape
+    width, rows = gate.shape
     mine = tok.shape[0] // (ny * NC)
     whole = width // LANES * LANES
     rest = width - whole
+    ahead = pa.shape[3]
     shard = wgs.shape[0]
     group = nx * shard
     scale = float(rows * nz * nx) ** (-0.5)
@@ -165,8 +166,7 @@
     wb[fs, :, whole:] = jnp.concatenate(
         [wvs[:, whole:].astype(F32), wgs[:, whole:].astype(F32)], axis=1
     ).astype(BF16)
-    later[...] = jnp.zeros_like(later)
-    terms[...] = jnp.zeros_like(terms)
+    terms[:, width:] = jnp.zeros((4, terms.shape[1] - width, LANES), F32)
     pl.semaphore_wait(barrier, len(peers))
 
     plan = Plan()
@@ -268,18 +268,27 @@
 
     offsets_z = [0] + [s * h for h in range(1, nz // 2) for s in (-1, 1)] + [nz // 2]
 
+    offsets_x = [0] + [s * h for h in range(1, nx // 2) for s in (-1, 1)] + [nx // 2]
+    az_first, az_ends = {}, {}
+    for r in offsets_x:
+        col = (x + r + nx) % nx
+        az_first[r], az_ends[r] = gather(
+            f"waz{r}",
+            "z",
+            lambda i, col=col: wa.at[i * nx + col],
+            lambda i, h, col=col: wa.at[i * nx + col, pl.ds(h * shard // 2, shard // 2)],
+            1,
+        )
     ax_first, ax_ends = gather(
-        "wax", "x", lambda i: wa.at[z * nx + i], lambda i, h: wa.at[z * nx + i, pl.ds(h * shard // 2, shard // 2)], 0
-    )
-    az_first, az_ends = gather(
-        "waz",
-        "z",
-        lambda i: wa.at[pl.ds(i * nx, nx)],
-        lambda i, h: wa.at[pl.ds(i * nx + h * (nx // 2), nx // 2)],
-        1,
-    )
-    plan.task("waz.go", 0, 0.02, after=[t for t in ax_ends.values() if t], sends=az_first)
-    az_ends[0] = "waz.go"
+        "wax",
+        "x",
+        lambda i: wa.at[z * nx + i],
+        lambda i, h: wa.at[z * nx + i, pl.ds(h * shard // 2, shard // 2)],
+        0,
+        extra=lambda r: az_first[r],
+    )
+    for r in offsets_x:
+        az_ends[r][0] = ax_ends[r]
     bx_first, bx_ends = {}, {}
     for d in offsets_z:
         bx_first[d], bx_ends[d] = gather(
@@ -313,7 +322,7 @@
         extra=lambda d: [f"twin{d}"],
     )
     plan.task("tok.own", 0, 0.02, lambda: loads["tok"].wait(), sends=tok_first + ["twin0"])
-    plan.task("go", -1, 0.02, sends=ax_first + bz_first + bx_first[0])
+    plan.task("go", -1, 0.02, sends=ax_first + bz_first + bx_first[0] + az_first[0])
     plan.task(
         "tok.all",
         3,
@@ -325,70 +334,65 @@
     k0 = 0.7978845608028654
     k1 = k0 * 0.044715
 
-    def act_step(row, col, size, write):
-        r = pl.ds(row, SUB)
-        cols = pl.ds(col, size)
-        g = gate[r, cols].astype(F32)
-        before = gate[pl.ds(pl.multiple_of(jnp.maximum(row - 16, 0), 16), 16), cols].astype(F32)[8:]
-        before = jnp.where(row > 0, before, 0.0)
-        both = jnp.concatenate([before, g], axis=0)
-        one = pltpu.roll(both, 1, 0)[8:]
-        two = pltpu.roll(both, 2, 0)[8:]
-        w0, w1, w2 = cw[0:1, cols], cw[1:2, cols], cw[2:3, cols]
-        conv = cb[0:1, cols] + w0 * two + w1 * one + w2 * g
+    lane = lax.broadcasted_iota(jnp.int32, (SUB, LANES), 1)
+
+    def shifted(value, by):
+        turned = pltpu.roll(value, by % rows, 1)
+        if by > 0:
+            edge = jnp.where(lane < by, 0.0, turned[:, :LANES])
+            return jnp.concatenate([edge, turned[:, LANES:]], axis=1)
+        edge = jnp.where(lane >= LANES + by, 0.0, turned[:, rows - LANES :])
+        return jnp.concatenate([turned[:, : rows - LANES], edge], axis=1)
+
+    def act_step(i):
+        units = pl.ds(pl.multiple_of(i * SUB, SUB), SUB)
+        g = gate[units, :].astype(F32)
+        one, two = shifted(g, 1), shifted(g, 2)
+        w0, w1, w2 = coef[units, 0:1], coef[units, 1:2], coef[units, 2:3]
+        conv = coef[units, 3:4] + w0 * two + w1 * one + w2 * g
         square = conv * conv
         t = jnp.tanh(conv * (k0 + k1 * square))
         cdf = 0.5 + 0.5 * t
         slope = cdf + conv * (0.5 - 0.5 * (t * t)) * (k0 + (3.0 * k1) * square)
-        hg = hidden[r, cols].astype(F32)
-        vg = hg * (conv * cdf)
-        cg = slope * (hg * value[r, cols].astype(F32))
-        after = jnp.concatenate([cg, later[:, cols]], axis=0)
-        gg = (
-            w2 * cg
-            + w1 * pltpu.roll(after, SUB + 7, 0)[:SUB]
-            + w0 * pltpu.roll(after, SUB + 6, 0)[:SUB]
-        )
-        later[:, cols] = cg[:8]
+        hg = hidden[units, :].astype(F32)
+        cg = slope * (hg * value[units, :].astype(F32))
+        gg = w2 * cg + w1 * shifted(cg, -1) + w0 * shifted(cg, -2)
         for k, term in enumerate((cg * two, cg * one, cg * g, cg)):
-            terms[k, :, cols] += term.reshape(SUB // 8, 8, size).sum(axis=0)
-        write(r, cols, gg, vg)
-
-    def write_whole(r, cols, gg, vg):
-        ga[r, cols] = gg.astype(BF16)
-        gb[r, cols] = vg.astype(BF16)
-
-    def write_rest(r, cols, gg, vg):
-        gb[r, whole:] = jnp.concatenate([vg, gg], axis=1).astype(BF16)
-
-    n_act = 8 if rows >= 8 * SUB else rows // SUB
-    per_act = rows // n_act // SUB
+            total = term[:, :LANES]
+            for j in range(1, rows // LANES):
+                total = total + term[:, j * LANES : (j + 1) * LANES]
+            terms[k, units, :] = total
+        at = jnp.where(i * SUB < whole, i * SUB, i * SUB + width)
+        gt[pl.ds(pl.multiple_of(at, SUB), SUB), :] = gg.astype(BF16)
+        at = i * SUB + whole
+        gt[pl.ds(pl.multiple_of(at, SUB), SUB), :] = (hg * (conv * cdf)).astype(BF16)
+
+    n_act = 11
+    per_act = width // SUB // n_act
 
     def act(k):
         if k == 0:
             for name in ("gate", "value", "hidden", "cw", "cb"):
                 loads[name].wait()
-
-        def sub(i, carry):
-            row = pl.multiple_of(rows - (k * per_act + i + 1) * SUB, SUB)
-
-            def col(j, carry):
-                act_step(row, pl.multiple_of(j * LANES, LANES), LANES, write_whole)
-                return carry
-
-            lax.fori_loop(0, whole // LANES, col, 0)
-            act_step(row, whole, rest, write_rest)
+            taps[0:3, :width] = cw[...]
+            taps[3, :width] = cb[...]
+            coef[...] = taps[...].T
+
+        def step(i, carry):
+            act_step(k * per_act + i)
             return carry
 
-        lax.fori_loop(0, per_act, sub, 0)
+        lax.fori_loop(0, per_act, step, 0)
 
     for k in range(n_act):
-        plan.task(f"act{k}", 5, 1.1, functools.partial(act, k), after=[f"act{k - 1}"] if k else [])
+        plan.task(f"act{k}", 5, 0.8, functools.partial(act, k), after=[f"act{k - 1}"] if k else [])
     acted = f"act{n_act - 1}"
 
+    pad = taps.shape[1]
+
     def conv_start():
-        sums = [terms[k].sum(axis=0, keepdims=True) for k in range(4)]
-        cx[x] = jnp.concatenate(sums + [jnp.zeros((4, width), F32)], axis=0)
+        sums = jnp.concatenate([terms[k].T.sum(axis=0, keepdims=True) for k in range(4)], axis=0)
+        cx[x] = jnp.concatenate([sums[:, : pad // 2], sums[:, pad // 2 :]], axis=0)
 
     def ring_of_slots(name, axis, slots):
         n, me, to = ring_at(axis)
@@ -420,8 +424,9 @@
         for i in range(1, nz):
             total = total + cz[i]
         total = total * scale
+        total = jnp.concatenate([total[:4], total[4:]], axis=1)[:, :width]
         cwg_out[...] = total[:3]
-        cbg_out[...] = total[3:4]
+        cbg_out[...] = total[3]
 
     plan.task("conv.start", 6, 0.2, conv_start, after=[acted], sends=cx_first)
     plan.task("conv.middle", 6, 0.1, conv_middle, after=cx_names + ["conv.start"], sends=cz_first)
@@ -432,8 +437,8 @@
     def grad(d):
         to_z = (z + d + nz) % nz
         left = tok[:, pl.ds(pl.multiple_of(to_z * group, group), group)]
-        over_rows = (((0,), (0,)), ((), ()))
-        for right, out in ((ga, pa), (gb, pb)):
+        over_rows = (((0,), (1,)), ((), ()))
+        for right, out in ((gt.at[:ahead], pa), (gt.at[ahead:], pb)):
             part = lax.dot_general(left, right[...], over_rows, preferred_element_type=F32)
             out[to_z] = part.astype(BF16).reshape(nx, shard, part.shape[1])
 
@@ -441,10 +446,10 @@
         plan.task(f"grad{d}", 7, 1.1, functools.partial(grad, d), after=["tok.all", acted])
 
     def ax_last(total):
-        gg_out[:, :whole] = total * scale
-
-    def az_last(total):
-        pa[z] = total.astype(BF16)
+        gg_out[:, :ahead] = total * scale
+
+    def az_last(r, total):
+        pa[z, (x + r + nx) % nx] = total.astype(BF16)
 
     scatter(
         "pax",
@@ -456,27 +461,31 @@
         lambda ref, j, h: ref.at[j, pl.ds(h * shard // 2, shard // 2)],
         3,
         0.1,
-        lambda d: ["paz.end"],
+        lambda d: [f"paz{d}.end"],
         ax_last,
     )
-    scatter(
-        "paz",
-        "z",
-        lambda i: pa.at[i],
-        lambda i, h: pa.at[i, pl.ds(h * (nx // 2), nx // 2)],
-        az_up,
-        az_dn,
-        lambda ref, j, h: ref.at[j, pl.ds(h * (nx // 2), nx // 2)],
-        2,
-        0.25,
-        lambda d: [f"grad{d}"],
-        az_last,
-    )
+    for i, r in enumerate([nx // 2] + [s * h for h in range(nx // 2 - 1, 0, -1) for s in (1, -1)] + [0]):
+        col = (x + r + nx) % nx
+        scatter(
+            f"paz{r}",
+            "z",
+            lambda i, col=col: pa.at[i, col],
+            lambda i, h, col=col: pa.at[i, col, pl.ds(h * shard // 2, shard // 2)],
+            az_up.at[i],
+            az_dn.at[i],
+            lambda ref, j, h: ref.at[j, pl.ds(h * shard // 2, shard // 2)],
+            2,
+            0.1,
+            lambda d: [f"grad{d}"],
+            functools.partial(az_last, r),
+        )
 
     def bz_last(total):
         total = total * scale
-        vg_out[...] = total[:, :width]
-        gg_out[:, whole:] = total[:, width:]
+        start = whole - ahead
+        gg_out[:, ahead:whole] = total[:, :start]
+        vg_out[...] = total[:, start : start + width]
+        gg_out[:, whole:] = total[:, start + width :]
 
     def bx_last(d, total):
         pb[(z + d + nz) % nz, x] = total.astype(BF16)
@@ -509,24 +518,24 @@
         bz_last,
     )
 
-    over_cols = (((1,), (1,)), ((), ()))
 
     def ig(d):
         at = (z + d + nz) % nz
         left_w = wa[pl.ds(at * nx, nx)].reshape(group, whole)
         right_w = wb[pl.ds(at * nx, nx)].reshape(group, 2 * width - whole)
-        part = lax.dot_general(ga[...], left_w, over_cols, preferred_element_type=F32)
-        part = part + lax.dot_general(gb[...], right_w, over_cols, preferred_element_type=F32)
+        part = jnp.dot(left_w, gt[:whole], preferred_element_type=F32)
+        part = part + jnp.dot(right_w, gt[whole:], preferred_element_type=F32)
         part = part.astype(BF16)
         for k in range(ny * NC):
-            igp[at, k % NC, k // NC] = part[k * mine : (k + 1) * mine]
+            igp[at, k % NC, k // NC] = part[:, k * mine : (k + 1) * mine]
 
     for d in offsets_z:
         at = (z + d + nz) % nz
         m = f"igt{d}"
         source, target = igp.at[at, 1 - c], twin_in.at[at]
         plan.message(m, "twin", source, target, twin, nbytes_of(source))
-        ends = [t for t in (az_ends[d], bz_ends[d], *bx_ends[d].values()) if t]
+        ends = [a[d] for a in az_ends.values()] + [bz_ends[d], *bx_ends[d].values()]
+        ends = [t for t in ends if t]
         plan.task(f"ig{d}", 8, 1.1, functools.partial(ig, d), after=[acted] + ends, sends=[m])
 
         def merge(at=at):
@@ -535,16 +544,16 @@
         plan.task(f"igm{d}", 3, 0.2, merge, waits=[m], after=[f"ig{d}"])
 
         def ig_last(total, at=at):
-            ig_out[:, pl.ds(pl.multiple_of(at * group, group), group)] = total.astype(BF16)
+            ig_out[:, pl.ds(pl.multiple_of(at * group, group), group)] = total.T.astype(BF16)
 
         scatter(
             f"igy{d}",
             "y",
             lambda i, at=at: igp.at[at, c, i],
-            lambda i, h, at=at: igp.at[at, c, i, pl.ds(h * (mine // 2), mine // 2)],
+            lambda i, h, at=at: igp.at[at, c, i, pl.ds(h * (group // 2), group // 2)],
             y_up.at[at],
             y_dn.at[at],
-            lambda ref, j, h: ref.at[j, pl.ds(h * (mine // 2), mine // 2)],
+            lambda ref, j, h: ref.at[j, pl.ds(h * (group // 2), group // 2)],
             3,
             0.05,
             lambda e, d=d: [f"igm{d}"],
@@ -583,68 +592,69 @@
     shard = up_gate_w.shape[0]
     whole = width // LANES * LANES
     ca, cb = whole, 2 * width - whole
+    pa, pb = whole - LANES, 2 * width - whole + LANES
+    pad = whole + LANES
     group = nx * shard
     shape = jax.ShapeDtypeStruct
-    out = pl.pallas_call(
+    return pl.pallas_call(
         functools.partial(kernel, dims),
         out_shape=(
             shape((mine, model), BF16),
             shape((shard, width), F32),
             shape((shard, width), F32),
             shape((3, width), F32),
-            shape((1, width), F32),
+            shape((width,), F32),
         ),
         in_specs=[pl.BlockSpec(memory_space=pl.ANY)] * 8,
         out_specs=[pl.BlockSpec(memory_space=pltpu.VMEM)] * 5,
         scratch_shapes=[
-            pltpu.VMEM((rows, width), BF16),
-            pltpu.VMEM((rows, width), BF16),
-            pltpu.VMEM((rows, width), BF16),
+            pltpu.VMEM((width, rows), BF16),
+            pltpu.VMEM((width, rows), BF16),
+            pltpu.VMEM((width, rows), BF16),
             pltpu.VMEM((shard, width), BF16),
             pltpu.VMEM((shard, width), BF16),
             pltpu.VMEM((3, width), F32),
-            pltpu.VMEM((1, width), F32),
+            pltpu.VMEM((width,), F32),
             pltpu.VMEM((mine * ny * NC, model), BF16),
             pltpu.VMEM((nz * nx, shard, ca), BF16),
             pltpu.VMEM((nz * nx, shard, cb), BF16),
-            pltpu.VMEM((rows, ca), BF16),
-            pltpu.VMEM((rows, cb), BF16),
-            pltpu.VMEM((nz, nx, shard, ca), BF16),
-            pltpu.VMEM((nz, nx, shard, cb), BF16),
-            pltpu.VMEM((nz // 2, nx, shard, ca), BF16),
-            pltpu.VMEM((nz // 2, nx, shard, ca), BF16),
-            pltpu.VMEM((nx // 2, shard, ca), BF16),
-            pltpu.VMEM((nx // 2, shard, ca), BF16),
-            pltpu.VMEM((nz, nx // 2, shard, cb), BF16),
-            pltpu.VMEM((nz, nx // 2, shard, cb), BF16),
-            pltpu.VMEM((nz // 2, shard, cb), BF16),
-            pltpu.VMEM((nz // 2, shard, cb), BF16),
-            pltpu.VMEM((nz, NC, ny, mine, group), BF16),
-            pltpu.VMEM((nz, ny, mine, group), BF16),
-            pltpu.VMEM((nz, ny // 2, mine, group), BF16),
-            pltpu.VMEM((nz, ny // 2, mine, group), BF16),
-            pltpu.VMEM((8, width), F32),
-            pltpu.VMEM((4, 8, width), F32),
-            pltpu.VMEM((nx, 8, width), F32),
-            pltpu.VMEM((nz, 8, width), F32),
+            pltpu.VMEM((2 * width, rows), BF16),
+            pltpu.VMEM((nz, nx, shard, pa), BF16),
+            pltpu.VMEM((nz, nx, shard, pb), BF16),
+            pltpu.VMEM((nx, nz // 2, shard, pa), BF16),
+            pltpu.VMEM((nx, nz // 2, shard, pa), BF16),
+            pltpu.VMEM((nx // 2, shard, pa), BF16),
+            pltpu.VMEM((nx // 2, shard, pa), BF16),
+            pltpu.VMEM((nz, nx // 2, shard, pb), BF16),
+            pltpu.VMEM((nz, nx // 2, shard, pb), BF16),
+            pltpu.VMEM((nz // 2, shard, pb), BF16),
+            pltpu.VMEM((nz // 2, shard, pb), BF16),
+            pltpu.VMEM((nz, NC, ny, group, mine), BF16),
+            pltpu.VMEM((nz, ny, group, mine), BF16),
+            pltpu.VMEM((nz, ny // 2, group, mine), BF16),
+            pltpu.VMEM((nz, ny // 2, group, mine), BF16),
+            pltpu.VMEM((8, pad), F32),
+            pltpu.VMEM((pad, 8), F32),
+            pltpu.VMEM((4, pad, LANES), F32),
+            pltpu.VMEM((nx, 8, pad // 2), F32),
+            pltpu.VMEM((nz, 8, pad // 2), F32),
             pltpu.SemaphoreType.DMA((8,)),
-            pltpu.SemaphoreType.DMA((192,)),
-            pltpu.SemaphoreType.DMA((192,)),
+            pltpu.SemaphoreType.DMA((224,)),
+            pltpu.SemaphoreType.DMA((224,)),
         ],
         compiler_params=pltpu.CompilerParams(
             collective_id=0, has_side_effects=True, vmem_limit_bytes=64_000_000
         ),
     )(
         tokens,
-        gate_pre,
-        value_pre,
+        gate_pre.T,
+        value_pre.T,
         up_gate_w,
         up_value_w,
         conv_weight,
-        conv_bias.reshape(1, width),
-        hidden_grad,
-    )
-    return (out[0], out[1], out[2], out[3], out[4].reshape(width))
+        conv_bias,
+        hidden_grad.T,
+    )
 
 
 def solution(mesh):

time: 104 us -> 87.5 us (0.84); the launches traced: 102 us -> 87.4 us
  Pallas kernels: 88.3 us -> 81.3 us
  local copies, waits for them, and re-layouts: 11.9 us -> 5.42 us
  other arithmetic: 1.32 us -> 0 us
    pallas_call x1, Pallas kernels: 88.3 us -> 81.3 us  [on_device(): pl.pallas_call(functools.partial(kernel, dims), out_shape=(shape((mine, m...]
    unnamed x15 -> x11, local copies, waits for them, and re-layouts: 10.5 us -> 5.42 us
    reshape x1 -> x0, local copies, waits for them, and re-layouts: 1.38 us -> none  [on_device(): conv_bias.reshape(1, width)]
    pallas_call x1 -> x0, other arithmetic: 1.32 us -> none  [on_device(): pl.pallas_call(functools.partial(kernel, dims), out_shape=(shape((mine, m...]
where the time goes in v2:
time: 87.5 us; the launch traced here: 87.4 us
  Pallas kernels  81.3 us (93%)
  local copies, waits for them, and re-layouts  5.42 us (6%)
    pallas_call x1, Pallas kernels, on_device(): pl.pallas_call(functools.partial(kernel, dims), out_shape=(shape((mine, m...  81.3 us
    unnamed x11, local copies, waits for them, and re-layouts  5.42 us

profile of v2, /device:TPU:8, one launch (start us, length us, event | category | flops | bytes accessed | tf_op | source)
XLA Modules:
  0.0 87.4 jit_solution(11485085539058403443)
XLA Ops:
  0.6 81.3 %shard_map.119 = (bf16[128,2048]{1,0:T(8,128)(2,1)}, f32[64,704]{1,0:T(8,128)}, f32[64,704]{1,0:T(8,128)}, f32[3,704]{1,0:T(4,128)}, f32[704]{0:T(1024)}) custom-call(bf16[128,2048]{1,0:T(8,128)(2,1)} %tokens.1, bf16[704,1024]{1,0:T(8,128)(2,1)} %bitcast.3, bf16[704,1024]{1,0:T(8,128)(2,1)} %bitcast.4, bf16[64,704]{1,0:T(8,128)(2,1)} %wg_in.1, ...), custom_call_target="tpu_custom_call" | custom-call | tf_op jit(solution)/shard_map/pallas_call | solution.py:599
  81.9 0.0 copy-start
  81.9 0.0 copy-start.1
  81.9 0.0 copy-start.2
  81.9 1.9 %copy.18 = bf16[128,2048]{1,0:T(8,128)(2,1)} copy(bf16[128,2048]{1,0:T(8,128)(2,1)} %get-tuple-element.10) | data formatting | bytes 1048576
  83.9 1.6 %copy.19 = f32[64,704]{1,0:T(8,128)} copy(f32[64,704]{1,0:T(8,128)} %get-tuple-element.11) | data formatting | bytes 360448
  85.5 0.0 copy-done
  85.5 0.7 copy.20
  86.2 0.0 copy-done.1
  86.2 0.6 copy.21
  86.8 0.0 copy-done.2
  86.8 0.6 copy.22
Async XLA Ops:
  81.9 3.6 %copy-start = (f32[64,704]{1,0:T(8,128)S(1)}, f32[64,704]{1,0:T(8,128)}, u32[]{:S(2)}) copy-start(f32[64,704]{1,0:T(8,128)} %get-tuple-element.12) | copy-start | bytes 540676
  81.9 4.2 %copy-start.1 = (f32[3,704]{1,0:T(4,128)S(1)}, f32[3,704]{1,0:T(4,128)}, u32[]{:S(2)}) copy-start(f32[3,704]{1,0:T(4,128)} %get-tuple-element.13) | copy-start | bytes 25348
  81.9 4.8 %copy-start.2 = (f32[704]{0:T(1024)S(1)}, f32[704]{0:T(1024)}, u32[]{:S(2)}) copy-start(f32[704]{0:T(1024)} %get-tuple-element.14) | copy-start | bytes 8452

commit v3 on v2

--- a/solution.py
+++ b/solution.py
@@ -14,49 +14,47 @@
 SUB = 16
 LANES = 128
 
-LINK = 46_650.0
-TWIN = 300_000.0
-HOP = 2.2
-TWIN_HOP = 1.0
+ORDER = (
+    41, 40, 43, 44, 45, 46, 34, 16, 47, 48, 0, 49, 50, 35, 51, 52, 17, 4, 20, 53,
+    38, 22, 8, 18, 60, 24, 1, 26, 36, 21, 12, 128, 23, 133, 19, 123, 129, 130, 9, 27,
+    39, 25, 5, 54, 134, 135, 2, 124, 125, 28, 37, 131, 42, 63, 74, 94, 30, 13, 65, 100,
+    64, 97, 84, 29, 70, 79, 10, 69, 95, 75, 31, 67, 106, 14, 6, 153, 98, 148, 80, 89,
+    101, 66, 154, 76, 96, 118, 103, 112, 132, 107, 155, 85, 68, 109, 32, 149, 150, 81, 136, 99,
+    55, 61, 126, 90, 138, 156, 77, 143, 151, 102, 119, 7, 139, 140, 104, 137, 15, 3, 115, 11,
+    86, 113, 144, 145, 127, 82, 56, 157, 108, 91, 152, 110, 78, 71, 141, 33, 158, 146, 105, 120,
+    159, 160, 87, 142, 116, 83, 57, 147, 114, 92, 161, 111, 121, 88, 72, 58, 162, 93, 117, 73,
+    122, 59, 62,
+)
 
 
 class Plan:
     def __init__(self):
         self.messages = {}
+        self.arrivals = {}
         self.tasks = {}
 
-    def message(self, name, link, source, target, device, nbytes):
-        self.messages[name] = (link, source, target, device, nbytes)
+    def message(self, name, link, source, target, device, arrival, group):
+        self.messages[name] = (link, source, target, device, arrival, group)
+        self.arrivals[arrival][1].append(name)
+
+    def arrival(self, name, whole):
+        self.arrivals[name] = (whole, [])
 
     def task(self, name, rank, cost, body=None, waits=(), after=(), sends=()):
         self.tasks[name] = (rank, cost, body, tuple(waits), tuple(after), tuple(sends))
 
     def order(self):
-        arrival, free, ended, listed = {}, {}, {}, []
-        left = dict(self.tasks)
-        now = 0.0
-        while left:
-            best = None
-            for name, (rank, cost, body, waits, after, sends) in left.items():
-                if any(w not in arrival for w in waits) or any(a not in ended for a in after):
-                    continue
-                ready = max([now] + [arrival[w] for w in waits])
-                key = (ready > now, ready if ready > now else 0.0, rank)
-                if best is None or key < best[0]:
-                    best = (key, name, ready)
-            name, ready = best[1], best[2]
-            rank, cost, body, waits, after, sends = left.pop(name)
-            now = ready + cost
-            ended[name] = now
-            listed.append(name)
-            for m in sends:
-                link, nbytes = self.messages[m][0], self.messages[m][4]
-                start = max(now, free.get(link, 0.0))
-                rate, hop = (TWIN, TWIN_HOP) if link == "twin" else (LINK, HOP)
-                free[link] = start + nbytes / rate
-                arrival[m] = free[link] + hop
-        self.length = now
-        self.ended = ended
+        names = list(self.tasks)
+        listed = [names[i] for i in ORDER]
+        assert sorted(listed) == sorted(names)
+        sent, done = set(), set()
+        for name in listed:
+            rank, cost, body, waits, after, sends = self.tasks[name]
+            assert all(m in sent for w in waits for m in self.arrivals[w][1]), name
+            assert all(a in done for a in after), name
+            sent.update(sends)
+            done.add(name)
+        assert sent == set(self.messages)
         return listed
 
 
@@ -123,7 +121,7 @@
     mine = tok.shape[0] // (ny * NC)
     whole = width // LANES * LANES
     rest = width - whole
-    ahead = pa.shape[3]
+    ahead = pa.shape[2]
     shard = wgs.shape[0]
     group = nx * shard
     scale = float(rows * nz * nx) ** (-0.5)
@@ -178,7 +176,7 @@
             "y": (ny, y, at_y),
         }[axis]
 
-    def gather(name, axis, block, half, rank, extra=None, first=None):
+    def gather(name, axis, block, half, pair, group, rank, extra=None, first=None):
         n, me, to = ring_at(axis)
         far = n // 2
 
@@ -188,31 +186,21 @@
         for h in range(1, far + 1):
             up, dn = idx(1 - h), idx(h - 1)
             su, sd = (block(up), block(dn)) if h < far else (half(up, 0), half(dn, 1))
-            plan.message(f"{name}.up{h}", axis + "+", su, su, to(1), nbytes_of(su))
-            plan.message(f"{name}.dn{h}", axis + "-", sd, sd, to(-1), nbytes_of(sd))
+            plan.arrival(f"{name}.{h}", pair if h < far else block(me))
+            plan.message(f"{name}.up{h}", axis + "+", su, su, to(1), f"{name}.{h}", group)
+            plan.message(f"{name}.dn{h}", axis + "-", sd, sd, to(-1), f"{name}.{h}", group)
         ends = {0: first}
-        for h in range(1, far):
-            for way, sign in (("up", -1), ("dn", 1)):
-                task = f"{name}.{way}{h}"
-                plan.task(
-                    task,
-                    rank,
-                    0.05,
-                    waits=[task],
-                    sends=[f"{name}.{way}{h + 1}"] + (extra(sign * h) if extra else []),
-                )
-                ends[sign * h] = task
-        plan.task(
-            f"{name}.last",
-            rank,
-            0.05,
-            waits=[f"{name}.up{far}", f"{name}.dn{far}"],
-            sends=extra(far) if extra else [],
-        )
-        ends[far] = f"{name}.last"
+        for h in range(1, far + 1):
+            sends = [f"{name}.up{h + 1}", f"{name}.dn{h + 1}"] if h < far else []
+            if extra:
+                sends += extra(-h) + extra(h) if h < far else extra(h)
+            plan.task(f"{name}.{h}", rank, 0.05, waits=[f"{name}.{h}"], sends=sends)
+            ends[h] = f"{name}.{h}"
+            if h < far:
+                ends[-h] = f"{name}.{h}"
         return [f"{name}.up1", f"{name}.dn1"], ends
 
-    def scatter(name, axis, block, half, up_in, dn_in, half_in, rank, cost, ready, last, then=()):
+    def scatter(name, axis, block, half, up_in, dn_in, half_in, pair, group, rank, cost, ready, last):
         n, me, to = ring_at(axis)
         far = n // 2
 
@@ -226,44 +214,39 @@
                 sd, td = half(dn, 1), half_in(dn_in, j - 1, 1)
             else:
                 su, tu, sd, td = block(up), up_in.at[j - 1], block(dn), dn_in.at[j - 1]
-            plan.message(f"{name}.up{j}", axis + "+", su, tu, to(1), nbytes_of(su))
-            plan.message(f"{name}.dn{j}", axis + "-", sd, td, to(-1), nbytes_of(sd))
+            plan.arrival(f"{name}.{j}", pair if j < far else block(me))
+            plan.message(f"{name}.up{j}", axis + "+", su, tu, to(1), f"{name}.{j}", group)
+            plan.message(f"{name}.dn{j}", axis + "-", sd, td, to(-1), f"{name}.{j}", group)
         plan.task(
             f"{name}.start", rank, 0.02, after=ready(far), sends=[f"{name}.up{far}", f"{name}.dn{far}"]
         )
+
+        def add(j):
+            for sign, h, came in ((1, 0, up_in), (-1, 1, dn_in)):
+                at = idx(sign * j)
+                if j + 1 == far:
+                    own, other = half(at, h), half_in(came, j, h)
+                else:
+                    own, other = block(at), came.at[j]
+                own[...] = (own[...].astype(F32) + other[...].astype(F32)).astype(BF16)
+
         for j in range(far - 1, 0, -1):
-            for way, sign, h, came in (("up", 1, 0, up_in), ("dn", -1, 1, dn_in)):
-                at = idx(sign * j)
-
-                def add(at=at, j=j, h=h, came=came):
-                    if j + 1 == far:
-                        own, other = half(at, h), half_in(came, j, h)
-                    else:
-                        own, other = block(at), came.at[j]
-                    own[...] = (own[...].astype(F32) + other[...].astype(F32)).astype(BF16)
-
-                plan.task(
-                    f"{name}.{way}{j}",
-                    rank,
-                    cost,
-                    add,
-                    waits=[f"{name}.{way}{j + 1}"],
-                    after=ready(sign * j),
-                    sends=[f"{name}.{way}{j}"],
-                )
+            plan.task(
+                f"{name}.{j}",
+                rank,
+                2 * cost,
+                functools.partial(add, j),
+                waits=[f"{name}.{j + 1}"],
+                after=ready(j) + ready(-j),
+                sends=[f"{name}.up{j}", f"{name}.dn{j}"],
+            )
         own = block(me)
 
         def end():
             last(own[...].astype(F32) + up_in[0].astype(F32) + dn_in[0].astype(F32))
 
         plan.task(
-            f"{name}.end",
-            rank,
-            cost * 1.5,
-            end,
-            waits=[f"{name}.up1", f"{name}.dn1"],
-            after=ready(0),
-            sends=then,
+            f"{name}.end", rank, cost * 1.5, end, waits=[f"{name}.1"], after=ready(0)
         )
 
     offsets_z = [0] + [s * h for h in range(1, nz // 2) for s in (-1, 1)] + [nz // 2]
@@ -277,6 +260,8 @@
             "z",
             lambda i, col=col: wa.at[i * nx + col],
             lambda i, h, col=col: wa.at[i * nx + col, pl.ds(h * shard // 2, shard // 2)],
+            wa.at[pl.ds(0, 2)],
+            "wa",
             1,
         )
     ax_first, ax_ends = gather(
@@ -284,6 +269,8 @@
         "x",
         lambda i: wa.at[z * nx + i],
         lambda i, h: wa.at[z * nx + i, pl.ds(h * shard // 2, shard // 2)],
+        wa.at[pl.ds(0, 2)],
+        "wa",
         0,
         extra=lambda r: az_first[r],
     )
@@ -296,6 +283,8 @@
             "x",
             lambda i, d=d: wb.at[((z + d + nz) % nz) * nx + i],
             lambda i, h, d=d: wb.at[((z + d + nz) % nz) * nx + i, pl.ds(h * shard // 2, shard // 2)],
+            wb.at[pl.ds(0, 2)],
+            "wb",
             2,
         )
     bz_first, bz_ends = gather(
@@ -303,6 +292,8 @@
         "z",
         lambda i: wb.at[i * nx + x],
         lambda i, h: wb.at[i * nx + x, pl.ds(h * shard // 2, shard // 2)],
+        wb.at[pl.ds(0, 2)],
+        "wb",
         0,
         extra=lambda d: bx_first[d],
     )
@@ -312,12 +303,15 @@
 
     for d in range(-(ny // 2) + 1, ny // 2 + 1):
         block = tok_at((y + d + ny) % ny)
-        plan.message(f"twin{d}", "twin", block, block, twin, nbytes_of(block))
+        plan.arrival(f"twin{d}", block)
+        plan.message(f"twin{d}", "twin", block, block, twin, f"twin{d}", "tok")
     tok_first, tok_ends = gather(
         "tok",
         "y",
         tok_at,
         lambda i, h: tok.at[pl.ds((i * NC + c) * mine + h * (mine // 2), mine // 2)],
+        tok.at[pl.ds(0, 2 * mine)],
+        "tok",
         0,
         extra=lambda d: [f"twin{d}"],
     )
@@ -385,7 +379,7 @@
         lax.fori_loop(0, per_act, step, 0)
 
     for k in range(n_act):
-        plan.task(f"act{k}", 5, 0.8, functools.partial(act, k), after=[f"act{k - 1}"] if k else [])
+        plan.task(f"act{k}", 5, 1.2, functools.partial(act, k), after=[f"act{k - 1}"] if k else [])
     acted = f"act{n_act - 1}"
 
     pad = taps.shape[1]
@@ -394,24 +388,21 @@
         sums = jnp.concatenate([terms[k].T.sum(axis=0, keepdims=True) for k in range(4)], axis=0)
         cx[x] = jnp.concatenate([sums[:, : pad // 2], sums[:, pad // 2 :]], axis=0)
 
-    def ring_of_slots(name, axis, slots):
-        n, me, to = ring_at(axis)
-        names = []
-        for h in range(1, n // 2 + 1):
-            for way, sign in (("up", 1), ("dn", -1)):
-                if h == n // 2 and sign < 0:
-                    continue
-                s = slots.at[(me + sign * (1 - h) + n) % n]
-                m = f"{name}.{way}{h}"
-                plan.message(m, axis + ("+" if sign > 0 else "-"), s, s, to(sign), nbytes_of(s))
-                nxt = [f"{name}.{way}{h + 1}"] if h + 1 < n // 2 or (h + 1 == n // 2 and sign > 0) else []
-                plan.task(m, 4, 0.05, waits=[m], sends=nxt)
-                names.append(m)
-        firsts = [f"{name}.up1"] + ([f"{name}.dn1"] if n > 2 else [])
-        return firsts, names
-
-    cx_first, cx_names = ring_of_slots("cx", "x", cx)
-    cz_first, cz_names = ring_of_slots("cz", "z", cz)
+    def slots_ring(name, axis, slots):
+        return gather(
+            name,
+            axis,
+            lambda i: slots.at[i],
+            lambda i, h: slots.at[i, :, pl.ds(h * 2 * LANES, (2 - h) * LANES)],
+            slots.at[pl.ds(0, 2)],
+            name,
+            4,
+        )
+
+    cx_first, cx_ends = slots_ring("cx", "x", cx)
+    cz_first, cz_ends = slots_ring("cz", "z", cz)
+    cx_names = [t for t in cx_ends.values() if t]
+    cz_names = [t for t in cz_ends.values() if t]
 
     def conv_middle():
         total = cx[0]
@@ -440,25 +431,27 @@
         over_rows = (((0,), (1,)), ((), ()))
         for right, out in ((gt.at[:ahead], pa), (gt.at[ahead:], pb)):
             part = lax.dot_general(left, right[...], over_rows, preferred_element_type=F32)
-            out[to_z] = part.astype(BF16).reshape(nx, shard, part.shape[1])
+            out[pl.ds(to_z * nx, nx)] = part.astype(BF16).reshape(nx, shard, part.shape[1])
 
     for d in grad_order:
-        plan.task(f"grad{d}", 7, 1.1, functools.partial(grad, d), after=["tok.all", acted])
+        plan.task(f"grad{d}", 7, 1.2, functools.partial(grad, d), after=["tok.all", acted])
 
     def ax_last(total):
         gg_out[:, :ahead] = total * scale
 
     def az_last(r, total):
-        pa[z, (x + r + nx) % nx] = total.astype(BF16)
+        pa[z * nx + (x + r + nx) % nx] = total.astype(BF16)
 
     scatter(
         "pax",
         "x",
-        lambda i: pa.at[z, i],
-        lambda i, h: pa.at[z, i, pl.ds(h * shard // 2, shard // 2)],
+        lambda i: pa.at[z * nx + i],
+        lambda i, h: pa.at[z * nx + i, pl.ds(h * shard // 2, shard // 2)],
         ax_up,
         ax_dn,
         lambda ref, j, h: ref.at[j, pl.ds(h * shard // 2, shard // 2)],
+        pa.at[pl.ds(0, 2)],
+        "pa",
         3,
         0.1,
         lambda d: [f"paz{d}.end"],
@@ -469,11 +462,13 @@
         scatter(
             f"paz{r}",
             "z",
-            lambda i, col=col: pa.at[i, col],
-            lambda i, h, col=col: pa.at[i, col, pl.ds(h * shard // 2, shard // 2)],
+            lambda i, col=col: pa.at[i * nx + col],
+            lambda i, h, col=col: pa.at[i * nx + col, pl.ds(h * shard // 2, shard // 2)],
             az_up.at[i],
             az_dn.at[i],
             lambda ref, j, h: ref.at[j, pl.ds(h * shard // 2, shard // 2)],
+            pa.at[pl.ds(0, 2)],
+            "pa",
             2,
             0.1,
             lambda d: [f"grad{d}"],
@@ -488,17 +483,19 @@
         gg_out[:, whole:] = total[:, start + width :]
 
     def bx_last(d, total):
-        pb[(z + d + nz) % nz, x] = total.astype(BF16)
+        pb[((z + d + nz) % nz) * nx + x] = total.astype(BF16)
 
     for i, d in enumerate(grad_order):
         scatter(
             f"pbx{d}",
             "x",
-            lambda i, d=d: pb.at[(z + d + nz) % nz, i],
-            lambda i, h, d=d: pb.at[(z + d + nz) % nz, i, pl.ds(h * shard // 2, shard // 2)],
+            lambda i, d=d: pb.at[((z + d + nz) % nz) * nx + i],
+            lambda i, h, d=d: pb.at[((z + d + nz) % nz) * nx + i, pl.ds(h * shard // 2, shard // 2)],
             bx_up.at[i],
             bx_dn.at[i],
             lambda ref, j, h: ref.at[j, pl.ds(h * shard // 2, shard // 2)],
+            pb.at[pl.ds(0, 2)],
+            "pb",
             2,
             0.1,
             lambda e, d=d: [f"grad{d}"],
@@ -507,11 +504,13 @@
     scatter(
         "pbz",
         "z",
-        lambda i: pb.at[i, x],
-        lambda i, h: pb.at[i, x, pl.ds(h * shard // 2, shard // 2)],
+        lambda i: pb.at[i * nx + x],
+        lambda i, h: pb.at[i * nx + x, pl.ds(h * shard // 2, shard // 2)],
         bz_up,
         bz_dn,
         lambda ref, j, h: ref.at[j, pl.ds(h * shard // 2, shard // 2)],
+        pb.at[pl.ds(0, 2)],
+        "pb",
         2,
         0.1,
         lambda d: [f"pbx{d}.end"],
@@ -533,7 +532,8 @@
         at = (z + d + nz) % nz
         m = f"igt{d}"
         source, target = igp.at[at, 1 - c], twin_in.at[at]
-        plan.message(m, "twin", source, target, twin, nbytes_of(source))
+        plan.arrival(m, source)
+        plan.message(m, "twin", source, target, twin, m, "ig")
         ends = [a[d] for a in az_ends.values()] + [bz_ends[d], *bx_ends[d].values()]
         ends = [t for t in ends if t]
         plan.task(f"ig{d}", 8, 1.1, functools.partial(ig, d), after=[acted] + ends, sends=[m])
@@ -554,34 +554,62 @@
             y_up.at[at],
             y_dn.at[at],
             lambda ref, j, h: ref.at[j, pl.ds(h * (group // 2), group // 2)],
+            igp.at[0, 0, pl.ds(0, 2)],
+            "ig",
             3,
             0.05,
             lambda e, d=d: [f"igm{d}"],
             ig_last,
         )
 
-    copies = {}
-    number = {name: i for i, name in enumerate(plan.messages)}
-    for name, (link, source, target, device, size) in plan.messages.items():
-        i = number[name]
-        copies[name] = pltpu.make_async_remote_copy(
+    left_from = {
+        "wa": wa.at[pl.ds(0, nz * nx - 1)],
+        "wb": wb.at[pl.ds(0, nz * nx - 1)],
+        "tok": tok.at[pl.ds(0, (2 * ny - 1) * mine)],
+        "pa": pa.at[pl.ds(0, nz * nx - 1)],
+        "pb": pb.at[pl.ds(0, nz * nx - 1)],
+        "ig": igp.at[pl.ds(0, nz * (2 * ny - 1) // (NC * ny))],
+        "cx": cx.at[pl.ds(0, nx - 1)],
+        "cz": cz.at[pl.ds(0, nz - 1)],
+    }
+    send_at = {name: send_sem.at[i] for i, name in enumerate(left_from)}
+    recv_at = {name: recv_sem.at[i] for i, name in enumerate(plan.arrivals)}
+    assert len(recv_at) == recv_sem.shape[0] and len(send_at) == send_sem.shape[0]
+    for name, whole_ref in left_from.items():
+        sizes = [nbytes_of(v[1]) for v in plan.messages.values() if v[5] == name]
+        assert sum(sizes) == nbytes_of(whole_ref), name
+
+    def remote(source, target, device, sent, arrival):
+        return pltpu.make_async_remote_copy(
             src_ref=source,
             dst_ref=target,
-            send_sem=send_sem.at[i],
-            recv_sem=recv_sem.at[i],
+            send_sem=send_at[sent],
+            recv_sem=recv_at[arrival],
             device_id=device,
             device_id_type=MESH,
         )
+
+    for name, (whole_ref, names) in plan.arrivals.items():
+        assert sum(nbytes_of(plan.messages[m][2]) for m in names) == nbytes_of(whole_ref), name
     for name in plan.order():
         rank, cost, body, waits, after, sends = plan.tasks[name]
-        for m in waits:
-            copies[m].wait_recv()
+        for w in waits:
+            ref, names = plan.arrivals[w]
+            remote(ref, ref, twin, plan.messages[names[0]][5], w).wait_recv()
         if body is not None:
             body()
         for m in sends:
-            copies[m].start()
-    for m in plan.messages:
-        copies[m].wait_send()
+            remote(*plan.messages[m][1:4], plan.messages[m][5], plan.messages[m][4]).start()
+    for name, ref in left_from.items():
+        remote(ref, ref, twin, name, next(iter(recv_at))).wait_send()
+
+
+def put_out(*refs):
+    copies = [pltpu.make_async_copy(refs[i], refs[5 + i], refs[10].at[i]) for i in range(5)]
+    for copy in copies:
+        copy.start()
+    for copy in copies:
+        copy.wait()
 
 
 def on_device(dims, *args):
@@ -595,17 +623,18 @@
     pa, pb = whole - LANES, 2 * width - whole + LANES
     pad = whole + LANES
     group = nx * shard
-    shape = jax.ShapeDtypeStruct
-    return pl.pallas_call(
+    n_arrivals = (3 + 2 * nz) * (nx // 2) + (3 + 2 * nx) * (nz // 2) + (nz + 1) * (ny // 2) + ny + nz
+    outs = (
+        ((mine, model), BF16),
+        ((shard, width), F32),
+        ((shard, width), F32),
+        ((3, width), F32),
+        ((width,), F32),
+    )
+    results = pl.pallas_call(
         functools.partial(kernel, dims),
-        out_shape=(
-            shape((mine, model), BF16),
-            shape((shard, width), F32),
-            shape((shard, width), F32),
-            shape((3, width), F32),
-            shape((width,), F32),
-        ),
-        in_specs=[pl.BlockSpec(memory_space=pl.ANY)] * 8,
+        out_shape=[pltpu.VMEM(*out) for out in outs],
+        in_specs=[pl.BlockSpec(memory_space=pltpu.HBM)] * 8,
         out_specs=[pl.BlockSpec(memory_space=pltpu.VMEM)] * 5,
         scratch_shapes=[
             pltpu.VMEM((width, rows), BF16),
@@ -619,8 +648,8 @@
             pltpu.VMEM((nz * nx, shard, ca), BF16),
             pltpu.VMEM((nz * nx, shard, cb), BF16),
             pltpu.VMEM((2 * width, rows), BF16),
-            pltpu.VMEM((nz, nx, shard, pa), BF16),
-            pltpu.VMEM((nz, nx, shard, pb), BF16),
+            pltpu.VMEM((nz * nx, shard, pa), BF16),
+            pltpu.VMEM((nz * nx, shard, pb), BF16),
             pltpu.VMEM((nx, nz // 2, shard, pa), BF16),
             pltpu.VMEM((nx, nz // 2, shard, pa), BF16),
             pltpu.VMEM((nx // 2, shard, pa), BF16),
@@ -639,22 +668,34 @@
             pltpu.VMEM((nx, 8, pad // 2), F32),
             pltpu.VMEM((nz, 8, pad // 2), F32),
             pltpu.SemaphoreType.DMA((8,)),
-            pltpu.SemaphoreType.DMA((224,)),
-            pltpu.SemaphoreType.DMA((224,)),
+            pltpu.SemaphoreType.DMA((8,)),
+            pltpu.SemaphoreType.DMA((n_arrivals,)),
         ],
         compiler_params=pltpu.CompilerParams(
-            collective_id=0, has_side_effects=True, vmem_limit_bytes=64_000_000
+            collective_id=0, has_side_effects=True, vmem_limit_bytes=56_000_000
         ),
     )(
-        tokens,
-        gate_pre.T,
-        value_pre.T,
-        up_gate_w,
-        up_value_w,
-        conv_weight,
-        conv_bias,
-        hidden_grad.T,
-    )
+        *(
+            pltpu.with_memory_space_constraint(a, pltpu.HBM)
+            for a in (
+                tokens,
+                gate_pre.T,
+                value_pre.T,
+                up_gate_w,
+                up_value_w,
+                conv_weight,
+                conv_bias,
+                hidden_grad.T,
+            )
+        )
+    )
+    return pl.pallas_call(
+        put_out,
+        out_shape=[jax.ShapeDtypeStruct(*out) for out in outs],
+        in_specs=[pl.BlockSpec(memory_space=pltpu.VMEM)] * 5,
+        out_specs=[pl.BlockSpec(memory_space=pltpu.HBM)] * 5,
+        scratch_shapes=[pltpu.SemaphoreType.DMA((5,))],
+    )(*(pltpu.with_memory_space_constraint(r, pltpu.VMEM) for r in results))
 
 
 def solution(mesh):

time: 87.5 us -> 75.9 us (0.87)
  Pallas kernels: 81.3 us -> 74.9 us
  local copies, waits for them, and re-layouts: 5.42 us -> 0 us
    pallas_call x1 -> x2, Pallas kernels: 81.3 us -> 74.9 us  [the longest x1 73.9 us: on_device(): pl.pallas_call(functools.partial(kernel, dims), out_shape=[pltpu.VMEM(*ou...]
    unnamed x11 -> x0, local copies, waits for them, and re-layouts: 5.42 us -> none
where the time goes in v3:
time: 75.9 us; the launch traced here: 75.7 us
  Pallas kernels  74.9 us (99%)
  between operations  0.82 us (1%)
    pallas_call x1, Pallas kernels, on_device(): pl.pallas_call(functools.partial(kernel, dims), out_shape=[pltpu.VMEM(*ou...  73.9 us

profile of v3, /device:TPU:8, one launch (start us, length us, event | category | flops | bytes accessed | tf_op | source)
XLA Modules:
  0.0 75.7 jit_solution(15815223830004861969)
XLA Ops:
  0.6 73.9 %shard_map.119 = (bf16[128,2048]{1,0:T(8,128)(2,1)S(1)}, f32[64,704]{1,0:T(8,128)S(1)}, f32[64,704]{1,0:T(8,128)S(1)}, f32[3,704]{1,0:T(4,128)S(1)}, f32[704]{0:T(1024)S(1)}) custom-call(bf16[128,2048]{1,0:T(8,128)(2,1)} %tokens.1, bf16[704,1024]{1,0:T(8,128)(2,1)} %bitcast.3, bf16[704,1024]{1,0:T(8,128)(2,1)} %bitcast.4, bf16[64,704]{1,0:T(8,128)(2,1)} %wg_in.1, ...), custom_call_target="tpu_custom_call" | custom-call | tf_op jit(solution)/shard_map/pallas_call | solution.py:634
  74.6 1.0 %shard_map.120 = (bf16[128,2048]{1,0:T(8,128)(2,1)}, f32[64,704]{1,0:T(8,128)}, f32[64,704]{1,0:T(8,128)}, f32[3,704]{1,0:T(4,128)}, f32[704]{0:T(1024)}) custom-call(bf16[128,2048]{1,0:T(8,128)(2,1)S(1)} %get-tuple-element.10.refs_0_, f32[64,704]{1,0:T(8,128)S(1)} %get-tuple-element.11.refs_1_, f32[64,704]{1,0:T(8,128)S(1)} %get-tuple-element.12.refs_2_, ...), custom_call_target="tpu_custom_call" | custom-call | tf_op jit(solution)/shard_map/pallas_call | solution.py:692

commit v4 on v3

--- a/solution.py
+++ b/solution.py
@@ -15,15 +15,15 @@
 LANES = 128
 
 ORDER = (
-    41, 40, 43, 44, 45, 46, 34, 16, 47, 48, 0, 49, 50, 35, 51, 52, 17, 4, 20, 53,
-    38, 22, 8, 18, 60, 24, 1, 26, 36, 21, 12, 128, 23, 133, 19, 123, 129, 130, 9, 27,
-    39, 25, 5, 54, 134, 135, 2, 124, 125, 28, 37, 131, 42, 63, 74, 94, 30, 13, 65, 100,
-    64, 97, 84, 29, 70, 79, 10, 69, 95, 75, 31, 67, 106, 14, 6, 153, 98, 148, 80, 89,
-    101, 66, 154, 76, 96, 118, 103, 112, 132, 107, 155, 85, 68, 109, 32, 149, 150, 81, 136, 99,
-    55, 61, 126, 90, 138, 156, 77, 143, 151, 102, 119, 7, 139, 140, 104, 137, 15, 3, 115, 11,
-    86, 113, 144, 145, 127, 82, 56, 157, 108, 91, 152, 110, 78, 71, 141, 33, 158, 146, 105, 120,
-    159, 160, 87, 142, 116, 83, 57, 147, 114, 92, 161, 111, 121, 88, 72, 58, 162, 93, 117, 73,
-    122, 59, 62,
+    41, 40, 43, 44, 45, 46, 34, 16, 47, 48, 0, 49, 50, 20, 35, 51, 52, 22, 17, 53,
+    8, 38, 62, 4, 21, 18, 1, 24, 36, 26, 12, 131, 23, 136, 19, 126, 132, 133, 25, 5,
+    54, 9, 39, 137, 138, 28, 2, 127, 128, 37, 134, 30, 42, 66, 77, 82, 55, 13, 97, 63,
+    87, 68, 103, 29, 6, 70, 109, 67, 100, 27, 72, 78, 98, 83, 69, 104, 106, 3, 14, 71,
+    56, 92, 10, 151, 101, 7, 31, 156, 79, 99, 121, 135, 32, 152, 153, 84, 88, 146, 57, 93,
+    15, 157, 158, 105, 112, 115, 141, 154, 107, 147, 11, 80, 148, 129, 139, 110, 73, 159, 118, 102,
+    142, 143, 122, 85, 33, 161, 155, 113, 58, 89, 149, 116, 130, 94, 162, 163, 140, 81, 74, 108,
+    160, 144, 111, 123, 150, 86, 164, 59, 64, 119, 90, 145, 95, 114, 165, 117, 124, 60, 91, 75,
+    96, 120, 61, 65, 125, 76,
 )
 
 
@@ -110,6 +110,8 @@
     terms,
     cx,
     cz,
+    ct,
+    csum,
     load_sem,
     send_sem,
     recv_sem,
@@ -188,10 +190,11 @@
             su, sd = (block(up), block(dn)) if h < far else (half(up, 0), half(dn, 1))
             plan.arrival(f"{name}.{h}", pair if h < far else block(me))
             plan.message(f"{name}.up{h}", axis + "+", su, su, to(1), f"{name}.{h}", group)
-            plan.message(f"{name}.dn{h}", axis + "-", sd, sd, to(-1), f"{name}.{h}", group)
+            if sd is not None:
+                plan.message(f"{name}.dn{h}", axis + "-", sd, sd, to(-1), f"{name}.{h}", group)
         ends = {0: first}
         for h in range(1, far + 1):
-            sends = [f"{name}.up{h + 1}", f"{name}.dn{h + 1}"] if h < far else []
+            sends = [m for m in (f"{name}.up{h + 1}", f"{name}.dn{h + 1}") if m in plan.messages]
             if extra:
                 sends += extra(-h) + extra(h) if h < far else extra(h)
             plan.task(f"{name}.{h}", rank, 0.05, waits=[f"{name}.{h}"], sends=sends)
@@ -389,39 +392,42 @@
         cx[x] = jnp.concatenate([sums[:, : pad // 2], sums[:, pad // 2 :]], axis=0)
 
     def slots_ring(name, axis, slots):
-        return gather(
-            name,
-            axis,
-            lambda i: slots.at[i],
-            lambda i, h: slots.at[i, :, pl.ds(h * 2 * LANES, (2 - h) * LANES)],
-            slots.at[pl.ds(0, 2)],
-            name,
-            4,
-        )
-
-    cx_first, cx_ends = slots_ring("cx", "x", cx)
-    cz_first, cz_ends = slots_ring("cz", "z", cz)
-    cx_names = [t for t in cx_ends.values() if t]
-    cz_names = [t for t in cz_ends.values() if t]
+        pair = slots.at[pl.ds(0, 2)]
+        first, ends = gather(
+            name, axis, lambda i: slots.at[i], lambda i, h: None if h else slots.at[i], pair, name, 4
+        )
+        return first, [t for t in ends.values() if t]
+
+    cx_first, cx_names = slots_ring("cx", "x", cx)
+    cz_first, cz_names = slots_ring("cz", "z", cz)
+    ct_first, ct_names = slots_ring("ct", "x", ct)
+    tiles = pad // 2 // LANES
+
+    def total_of(slots, n):
+        total = slots[0]
+        for i in range(1, n):
+            total = total + slots[i]
+        return total
 
     def conv_middle():
-        total = cx[0]
-        for i in range(1, nx):
-            total = total + cx[i]
-        cz[z] = total
+        total = total_of(cx, nx)
+        for j in range(tiles):
+            csum[j] = total[:, j * LANES : (j + 1) * LANES]
+        cz[z] = csum[jnp.minimum(x, tiles - 1)]
+
+    def conv_late():
+        ct[x] = total_of(cz, nz)
 
     def conv_end():
-        total = cz[0]
-        for i in range(1, nz):
-            total = total + cz[i]
-        total = total * scale
+        total = jnp.concatenate([ct[j] for j in range(tiles)], axis=1) * scale
         total = jnp.concatenate([total[:4], total[4:]], axis=1)[:, :width]
         cwg_out[...] = total[:3]
         cbg_out[...] = total[3]
 
     plan.task("conv.start", 6, 0.2, conv_start, after=[acted], sends=cx_first)
     plan.task("conv.middle", 6, 0.1, conv_middle, after=cx_names + ["conv.start"], sends=cz_first)
-    plan.task("conv.end", 9, 0.1, conv_end, after=cz_names + ["conv.middle"])
+    plan.task("conv.late", 6, 0.1, conv_late, after=cz_names + ["conv.middle"], sends=ct_first)
+    plan.task("conv.end", 9, 0.1, conv_end, after=ct_names + ["conv.late"])
 
     grad_order = [nz // 2] + [s * h for h in range(nz // 2 - 1, 0, -1) for s in (1, -1)] + [0]
 
@@ -571,6 +577,7 @@
         "ig": igp.at[pl.ds(0, nz * (2 * ny - 1) // (NC * ny))],
         "cx": cx.at[pl.ds(0, nx - 1)],
         "cz": cz.at[pl.ds(0, nz - 1)],
+        "ct": ct.at[pl.ds(0, nx - 1)],
     }
     send_at = {name: send_sem.at[i] for i, name in enumerate(left_from)}
     recv_at = {name: recv_sem.at[i] for i, name in enumerate(plan.arrivals)}
@@ -623,7 +630,7 @@
     pa, pb = whole - LANES, 2 * width - whole + LANES
     pad = whole + LANES
     group = nx * shard
-    n_arrivals = (3 + 2 * nz) * (nx // 2) + (3 + 2 * nx) * (nz // 2) + (nz + 1) * (ny // 2) + ny + nz
+    n_arrivals = (4 + 2 * nz) * (nx // 2) + (3 + 2 * nx) * (nz // 2) + (nz + 1) * (ny // 2) + ny + nz
     outs = (
         ((mine, model), BF16),
         ((shard, width), F32),
@@ -666,9 +673,11 @@
             pltpu.VMEM((pad, 8), F32),
             pltpu.VMEM((4, pad, LANES), F32),
             pltpu.VMEM((nx, 8, pad // 2), F32),
-            pltpu.VMEM((nz, 8, pad // 2), F32),
+            pltpu.VMEM((nz, 8, LANES), F32),
+            pltpu.VMEM((nx, 8, LANES), F32),
+            pltpu.VMEM((pad // 2 // LANES, 8, LANES), F32),
             pltpu.SemaphoreType.DMA((8,)),
-            pltpu.SemaphoreType.DMA((8,)),
+            pltpu.SemaphoreType.DMA((9,)),
             pltpu.SemaphoreType.DMA((n_arrivals,)),
         ],
         compiler_params=pltpu.CompilerParams(

time: 75.9 us -> 75.2 us (level)
  no operation moved by 1% of the time
where the time goes in v4:
time: 75.2 us; the launch traced here: 75.1 us
  Pallas kernels  74.3 us (99%)
  between operations  0.82 us (1%)
    pallas_call x1, Pallas kernels, on_device(): pl.pallas_call(functools.partial(kernel, dims), out_shape=[pltpu.VMEM(*ou...  73.3 us

profile of v4, /device:TPU:8, one launch (start us, length us, event | category | flops | bytes accessed | tf_op | source)
XLA Modules:
  0.0 75.1 jit_solution(6859631764689301032)
XLA Ops:
  0.6 73.3 %shard_map.119 = (bf16[128,2048]{1,0:T(8,128)(2,1)S(1)}, f32[64,704]{1,0:T(8,128)S(1)}, f32[64,704]{1,0:T(8,128)S(1)}, f32[3,704]{1,0:T(4,128)S(1)}, f32[704]{0:T(1024)S(1)}) custom-call(bf16[128,2048]{1,0:T(8,128)(2,1)} %tokens.1, bf16[704,1024]{1,0:T(8,128)(2,1)} %bitcast.3, bf16[704,1024]{1,0:T(8,128)(2,1)} %bitcast.4, bf16[64,704]{1,0:T(8,128)(2,1)} %wg_in.1, ...), custom_call_target="tpu_custom_call" | custom-call | tf_op jit(solution)/shard_map/pallas_call | solution.py:641
  73.9 1.0 %shard_map.120 = (bf16[128,2048]{1,0:T(8,128)(2,1)}, f32[64,704]{1,0:T(8,128)}, f32[64,704]{1,0:T(8,128)}, f32[3,704]{1,0:T(4,128)}, f32[704]{0:T(1024)}) custom-call(bf16[128,2048]{1,0:T(8,128)(2,1)S(1)} %get-tuple-element.10.refs_0_, f32[64,704]{1,0:T(8,128)S(1)} %get-tuple-element.11.refs_1_, f32[64,704]{1,0:T(8,128)S(1)} %get-tuple-element.12.refs_2_, ...), custom_call_target="tpu_custom_call" | custom-call | tf_op jit(solution)/shard_map/pallas_call | solution.py:701

commit v5 on v4

--- a/solution.py
+++ b/solution.py
@@ -139,6 +139,10 @@
 
     twin = (fs, y * NC + 1 - c)
 
+    barrier = pltpu.get_barrier_semaphore()
+    peers = (at_z(1), at_z(-1), at_x(1), at_x(-1), at_y(1), at_y(-1), twin)
+    for peer in peers:
+        pl.semaphore_signal(barrier, inc=1, device_id=peer, device_id_type=MESH)
     loads = {}
     for i, (name, source, target) in enumerate(
         (
@@ -154,10 +158,6 @@
     ):
         loads[name] = pltpu.make_async_copy(source, target, load_sem.at[i])
         loads[name].start()
-    barrier = pltpu.get_barrier_semaphore()
-    peers = (at_z(1), at_z(-1), at_x(1), at_x(-1), at_y(1), at_y(-1), twin)
-    for peer in peers:
-        pl.semaphore_signal(barrier, inc=1, device_id=peer, device_id_type=MESH)
 
     loads["wg"].wait()
     loads["wv"].wait()
@@ -224,21 +224,22 @@
             f"{name}.start", rank, 0.02, after=ready(far), sends=[f"{name}.up{far}", f"{name}.dn{far}"]
         )
 
-        def add(j):
-            for sign, h, came in ((1, 0, up_in), (-1, 1, dn_in)):
+        def add(j, start):
+            for way, sign, h, came in (("up", 1, 0, up_in), ("dn", -1, 1, dn_in)):
                 at = idx(sign * j)
                 if j + 1 == far:
                     own, other = half(at, h), half_in(came, j, h)
                 else:
                     own, other = block(at), came.at[j]
                 own[...] = (own[...].astype(F32) + other[...].astype(F32)).astype(BF16)
+                start(f"{name}.{way}{j}")
 
         for j in range(far - 1, 0, -1):
             plan.task(
                 f"{name}.{j}",
                 rank,
                 2 * cost,
-                functools.partial(add, j),
+                (functools.partial(add, j),),
                 waits=[f"{name}.{j + 1}"],
                 after=ready(j) + ready(-j),
                 sends=[f"{name}.up{j}", f"{name}.dn{j}"],
@@ -598,15 +599,23 @@
 
     for name, (whole_ref, names) in plan.arrivals.items():
         assert sum(nbytes_of(plan.messages[m][2]) for m in names) == nbytes_of(whole_ref), name
+
+    def start(m):
+        link, source, target, device, arrival, sent = plan.messages[m]
+        remote(source, target, device, sent, arrival).start()
+
     for name in plan.order():
         rank, cost, body, waits, after, sends = plan.tasks[name]
         for w in waits:
             ref, names = plan.arrivals[w]
             remote(ref, ref, twin, plan.messages[names[0]][5], w).wait_recv()
+        if isinstance(body, tuple):
+            body[0](start)
+            continue
         if body is not None:
             body()
         for m in sends:
-            remote(*plan.messages[m][1:4], plan.messages[m][5], plan.messages[m][4]).start()
+            start(m)
     for name, ref in left_from.items():
         remote(ref, ref, twin, name, next(iter(recv_at))).wait_send()
 

time: 75.2 us -> 75.2 us (level)
  no operation moved by 1% of the time
where the time goes in v5:
time: 75.2 us; the launch traced here: 75.1 us
  Pallas kernels  74.3 us (99%)
  between operations  0.82 us (1%)
    pallas_call x1, Pallas kernels, on_device(): pl.pallas_call(functools.partial(kernel, dims), out_shape=[pltpu.VMEM(*ou...  73.3 us

profile of v5, /device:TPU:8, one launch (start us, length us, event | category | flops | bytes accessed | tf_op | source)
XLA Modules:
  0.0 75.1 jit_solution(1034918683088527801)
XLA Ops:
  0.6 73.3 %shard_map.119 = (bf16[128,2048]{1,0:T(8,128)(2,1)S(1)}, f32[64,704]{1,0:T(8,128)S(1)}, f32[64,704]{1,0:T(8,128)S(1)}, f32[3,704]{1,0:T(4,128)S(1)}, f32[704]{0:T(1024)S(1)}) custom-call(bf16[128,2048]{1,0:T(8,128)(2,1)} %tokens.1, bf16[704,1024]{1,0:T(8,128)(2,1)} %bitcast.3, bf16[704,1024]{1,0:T(8,128)(2,1)} %bitcast.4, bf16[64,704]{1,0:T(8,128)(2,1)} %wg_in.1, ...), custom_call_target="tpu_custom_call" | custom-call | tf_op jit(solution)/shard_map/pallas_call | solution.py:650
  73.9 1.0 %shard_map.120 = (bf16[128,2048]{1,0:T(8,128)(2,1)}, f32[64,704]{1,0:T(8,128)}, f32[64,704]{1,0:T(8,128)}, f32[3,704]{1,0:T(4,128)}, f32[704]{0:T(1024)}) custom-call(bf16[128,2048]{1,0:T(8,128)(2,1)S(1)} %get-tuple-element.10.refs_0_, f32[64,704]{1,0:T(8,128)S(1)} %get-tuple-element.11.refs_1_, f32[64,704]{1,0:T(8,128)S(1)} %get-tuple-element.12.refs_2_, ...), custom_call_target="tpu_custom_call" | custom-call | tf_op jit(solution)/shard_map/pallas_call | solution.py:710
